TPU v7x, 512 devices: a whole 4x8x8 slice. The times are simulated.
512 devices in a mesh: sp: 64 (over z, y), tp: 8 (over x, core).
Axes of the slice: x: 4, y: 8, z: 8, core: 2. Of those that a mesh axis runs over, the one named last changes fastest.
Arguments:
- tokens: bfloat16 [16384, 2048], P(('sp', 'tp')), may hold values from -6 to 6
- norm_gain: float32 [2048], replicated, may hold values from 0.1 to 1.9
- w_query: bfloat16 [2048, 1024], P('sp', 'tp'), may hold values from -0.125 to 0.125
- w_forget: bfloat16 [2048, 1024], P('sp', 'tp'), may hold values from -0.125 to 0.125
- w_input: bfloat16 [2048, 1024], P('sp', 'tp'), may hold values from -0.125 to 0.125
- w_outgate: bfloat16 [2048, 1024], P('sp', 'tp'), may hold values from -0.125 to 0.125
- w_bgate: bfloat16 [2048, 1024], P('sp', 'tp'), may hold values from -0.125 to 0.125
- w_cgate: bfloat16 [2048, 1024], P('sp', 'tp'), may hold values from -0.125 to 0.125
- w_value: bfloat16 [2048, 1024], P('sp', 'tp'), may hold values from -0.125 to 0.125
- floor_gap: float32 [8, 128], P('tp'), may hold values from 0 to 0.06
- extra_decay: float32 [16384, 8], P('sp', 'tp'), may hold values from -1 to 0
- start_state: float32 [8, 128, 128], P('tp'), may hold values from -0.02734375 to 0.02734375
- state_gain: float32 [128], replicated, may hold values from 0.1 to 1.9
- conv_taps: float32 [3, 1024], P(None, 'tp'), may hold values from -3 to 3
- out_rec: bfloat16 [1024, 2048], P('tp', 'sp'), may hold values from -0.125 to 0.125
- out_conv: bfloat16 [1024, 2048], P('tp', 'sp'), may hold values from -0.125 to 0.125
Outputs:
- mixed_sum: bfloat16 [16384, 2048], P(('sp', 'tp'))
All inputs are finite; a program needn't handle non-finite values.
Results may differ from a plain program's by a relative error of at most 0.018.
Values may be sent and summed in bfloat16 or wider, within the bound.
A program may use at most 64 MiB of HBM per device.

v0:
```python
import jax
import jax.numpy as jnp
from jax import lax
from jax.sharding import Mesh
from jax.sharding import PartitionSpec as P

BLOCK = 64
SP = ("sp_0", "sp_1")
TP = ("tp_0", "tp_1")
SP_TP = ("sp_0", "sp_1", "tp_0", "tp_1")


eps = 1e-06
highest_precision = lax.Precision.HIGHEST


def side_by_side(arrays, axis, dim, along):
    ends, at = ([], 0)
    for a in arrays[:-1]:
        at += a.shape[along]
        ends.append(at)
    both = jnp.concatenate(arrays, axis=along)
    return tuple(jnp.split(lax.all_gather(both, axis, axis=dim, tiled=True), ends, axis=along))


def edges_of(length, count):
    unit = 8 if length >= 8 * count else 1
    return [length // unit * k // count * unit for k in range(1, count)]


def stacked_from(value, axes, order):
    parts = value[None]
    for k in order:
        parts = lax.all_gather(parts, axes[k], axis=0, tiled=True)
    current = [lax.axis_size(axes[k]) for k in reversed(order)]
    parts = parts.reshape(*current, *value.shape)
    turned = sorted(range(len(order)), key=lambda place: order[len(order) - 1 - place])
    return parts.transpose(*turned, *range(len(order), parts.ndim)).reshape(-1, *value.shape)


def laid_out(parts, dim):
    parts = jnp.moveaxis(parts, 0, dim)
    dims = parts.shape
    return parts.reshape(*dims[:dim], dims[dim] * dims[dim + 1], *dims[dim + 2 :])


def gather_at_once(value, axes, dim):
    numbers = list(range(len(axes)))[::-1]
    widest = value.shape.index(max(value.shape[:-1] or value.shape))
    edges = [0, *edges_of(value.shape[widest], len(axes)), value.shape[widest]]
    done = []
    for k, (start, end) in enumerate(zip(edges, edges[1:])):
        if end > start:
            slab = lax.slice_in_dim(value, start, end, axis=widest)
            done.append(stacked_from(slab, axes, numbers[k:] + numbers[:k]))
    return laid_out(jnp.concatenate(done, axis=widest + 1), dim)


def nothing_yet(value, identity):
    return jax.tree.map(
        lambda part, zero: jnp.zeros_like(part) + jnp.asarray(zero, part.dtype), value, identity
    )


def all_in_one(value, axis):
    leaves = jax.tree.leaves(value)
    order = sorted(range(len(leaves)), key=lambda k: -leaves[k].size)
    width = (1, *leaves[order[0]].shape)[-1]
    lines = [
        jnp.pad(leaves[k].reshape(-1), (0, -leaves[k].size % width)).reshape(-1, width)
        for k in order
    ]
    both, at, found = (lax.all_gather(jnp.concatenate(lines), axis), 0, {})
    for k, line in zip(order, lines):
        slab = both[:, at : at + len(line)].reshape(len(both), -1)
        found[k] = slab[:, : leaves[k].size].reshape(-1, *leaves[k].shape)
        at += len(line)
    numbers = iter(range(len(leaves)))
    return jax.tree.map(lambda _: found[next(numbers)], value)


def carried_in(value, axes, combine, identity):
    before = start = nothing_yet(value, identity)
    so_far = value
    for axis in reversed(axes):
        count, mine = (lax.axis_size(axis), lax.axis_index(axis))
        pieces = all_in_one(so_far, axis)
        inside, so_far = (start, start)
        for k in range(count):
            passed = k < mine
            so_far = combine(so_far, jax.tree.map(lambda part: part[k], pieces))
            inside = jax.tree.map(lambda new, old: jnp.where(passed, new, old), so_far, inside)
        before = combine(inside, before)
    return before


def shifted(block, axis, distance):
    devices = range(lax.axis_size(axis))
    route = [(i - distance, i) for i in devices if i - distance in devices]
    return lax.ppermute(block, axis, route)


def turned_gather(arrays, axis, dims):
    turned = [jnp.moveaxis(a, dim, 0) for a, dim in zip(arrays, dims)]
    both = jnp.concatenate([t.reshape(len(t), -1) for t in turned], axis=1)
    whole, at, done = (lax.all_gather(both, axis, axis=0, tiled=True), 0, [])
    for t, dim in zip(turned, dims):
        slab = whole[:, at : at + t[0].size].reshape(-1, *t.shape[1:])
        done.append(jnp.moveaxis(slab, 0, dim))
        at += t[0].size
    return tuple(done)


def split_up(value, dim, count):
    before, after = (value.shape[:dim], value.shape[dim + 1 :])
    return jnp.moveaxis(value.reshape(*before, count, -1, *after), dim, 0)


def sum_at_owner(value, axis, dim):
    parts = split_up(value, dim, lax.axis_size(axis))
    arrived = lax.all_to_all(parts, axis, split_axis=0, concat_axis=0, tiled=True)
    return arrived.astype(jnp.float32).sum(axis=0)


def rms_scale(values):
    return lax.rsqrt(jnp.mean(values * values, axis=-1, keepdims=True) + eps)


def local_blocks(queries, write_in, inputs, log_keep, block_len):
    length, head_count, address_feature_count = queries.shape
    value_dim = inputs.shape[-1]
    blocks_count = length // block_len

    def blocked(tensor):
        return tensor.reshape(blocks_count, block_len, head_count, tensor.shape[-1]).transpose(
            0, 2, 1, 3
        )

    def unblock(tensor):
        return tensor.transpose(0, 2, 1, 3).reshape(length, head_count, tensor.shape[-1])

    causal = (jnp.arange(block_len)[:, None] >= jnp.arange(block_len)[None, :])[None, :, :, None]

    def advance(carried, pieces):
        memory_state, offset = carried
        query_block, write_blk, input_block, keep_blk = pieces
        running_state = jnp.cumsum(keep_blk, axis=1)
        spread = running_state[:, :, None, :] - running_state[:, None, :, :]
        decays = jnp.where(causal, jnp.exp(jnp.minimum(spread, 0.0)), 0.0)
        scores = jnp.sum(query_block[:, :, None, :] * write_blk[:, None, :, :] * decays, axis=-1)
        final_output = jnp.einsum(
            "qcp,qpi->qci",
            query_block * jnp.exp(running_state),
            memory_state,
            precision=highest_precision,
        )
        final_output = final_output + jnp.einsum(
            "hts,hsv->htv", scores, input_block, precision=highest_precision
        )
        lifted_state = query_block * jnp.exp(running_state + offset[:, None, :])
        final_state = running_state[:, -1, :]
        weighted_value = write_blk * jnp.exp(final_state[:, None, :] - running_state)
        memory_state = memory_state * jnp.exp(final_state)[:, :, None] + jnp.einsum(
            "euz,eul->ezl", weighted_value, input_block, precision=highest_precision
        )
        return ((memory_state, offset + final_state), (final_output, lifted_state))

    initial = (
        jnp.zeros((head_count, address_feature_count, value_dim), jnp.float32),
        jnp.zeros((head_count, address_feature_count), jnp.float32),
    )
    finals, outputs = lax.scan(
        advance, initial, (blocked(queries), blocked(write_in), blocked(inputs), blocked(log_keep))
    )
    return (unblock(outputs[0]), unblock(outputs[1]), finals[0], jnp.exp(finals[1]))


def chain(earlier, later):
    return (earlier[0] * later[0], earlier[1] * later[0][:, :, None] + later[1])


def on_device(
    tokens,
    norm_gain,
    w_query,
    w_forget,
    w_input,
    w_outgate,
    w_bgate,
    w_cgate,
    w_value,
    floor_gap,
    extra_decay,
    start_state,
    state_gain,
    conv_taps,
    out_rec,
    out_conv,
):
    tokens_f = tokens.astype(jnp.float32)
    normed = (tokens_f * rms_scale(tokens_f) * norm_gain).astype(jnp.bfloat16)
    weights = (w_query, w_forget, w_input, w_outgate, w_bgate, w_cgate, w_value)
    whole_weights = side_by_side(
        (w_query, w_forget, w_input, w_outgate, w_bgate, w_cgate, w_value), SP, 0, 1
    )

    def project(shard_rows):
        return jnp.concatenate(
            [
                jnp.dot(shard_rows, matrix, preferred_element_type=jnp.float32).astype(jnp.bfloat16)
                for matrix in whole_weights
            ],
            axis=1,
        )

    joined = project(gather_at_once(normed, TP, 0))
    borders = [0]
    for matrix in weights:
        borders.append(borders[-1] + matrix.shape[1])
    projected = [joined[:, borders[number] : borders[number + 1]] for number in range(len(weights))]
    query_raw, forget_raw, input_raw, outgate_raw, bgate_raw, cgate_raw, value_raw = projected
    length = query_raw.shape[0]
    head_count, address_feature_count = floor_gap.shape
    value_dim = start_state.shape[2]
    queries = jax.nn.silu(query_raw.astype(jnp.float32)).reshape(
        length, head_count, address_feature_count
    )
    write_in = floor_gap[None] * jax.nn.sigmoid(-forget_raw.astype(jnp.float32)).reshape(
        length, head_count, address_feature_count
    )
    log_keep = jnp.log1p(-write_in) + extra_decay[:, :, None]
    inputs = input_raw.astype(jnp.float32).reshape(length, head_count, value_dim)
    output_list, lifted_state, memory_state, kept = local_blocks(
        queries, write_in, inputs, log_keep, BLOCK
    )
    before_keep, before_memory = carried_in(
        (kept, memory_state), SP, chain, (jnp.ones_like(kept), jnp.zeros_like(memory_state))
    )
    carried_hidden_prior = start_state * before_keep[:, :, None] + before_memory
    blended_state = output_list + jnp.einsum(
        "sqa,qar->sqr", lifted_state, carried_hidden_prior, precision=highest_precision
    )
    gate_out = jax.nn.silu(outgate_raw.astype(jnp.float32)).reshape(length, head_count, value_dim)
    rec_out = (
        (blended_state * rms_scale(blended_state) * state_gain * gate_out)
        .reshape(length, head_count * value_dim)
        .astype(jnp.bfloat16)
    )
    rim_rows = jnp.stack([cgate_raw[length - 2 :], value_raw[length - 2 :]])
    before_rim = shifted(rim_rows, SP, 1)
    convolution_gate_widened = jnp.concatenate([before_rim[0], cgate_raw], axis=0).astype(
        jnp.float32
    )
    value_ext = jnp.concatenate([before_rim[1], value_raw], axis=0).astype(jnp.float32)
    gated = convolution_gate_widened * value_ext
    conv_out = (
        conv_taps[0] * gated[:length]
        + conv_taps[1] * gated[1 : length + 1]
        + conv_taps[2] * gated[2:]
    )
    short_out = (bgate_raw.astype(jnp.float32) * conv_out).astype(jnp.bfloat16)
    rec_weight, conv_weight = turned_gather((out_rec, out_conv), SP, (1, 1))
    product = jnp.dot(rec_out, rec_weight, preferred_element_type=jnp.float32)
    mixed_sum = sum_at_owner(
        (product + jnp.dot(short_out, conv_weight, preferred_element_type=jnp.float32)).astype(
            jnp.bfloat16
        ),
        TP,
        0,
    )
    return mixed_sum.astype(jnp.bfloat16)


def solution(mesh):
    torus = Mesh(mesh.devices.reshape(8, 8, 4, 2), ("sp_0", "sp_1", "tp_0", "tp_1"))
    return jax.shard_map(
        on_device,
        mesh=torus,
        in_specs=(
            P(SP_TP, None),
            P(),
            P(SP, TP),
            P(SP, TP),
            P(SP, TP),
            P(SP, TP),
            P(SP, TP),
            P(SP, TP),
            P(SP, TP),
            P(TP, None),
            P(SP, TP),
            P(TP, None, None),
            P(),
            P(None, TP),
            P(TP, SP),
            P(TP, SP),
        ),
        out_specs=P(SP_TP, None),
        check_vma=False,
    )
```

profile of v0, /device:TPU:1, one launch (start us, length us, event | category | flops | bytes accessed | tf_op | source)
XLA Modules:
  0.0 218.3 jit_solution(16532553705476174274)
XLA Ops:
  6.5 0.0 all-gather.9.cloned.1.call-start
  6.5 0.7 constant_dynamic-update-slice_fusion.6
  7.2 0.7 constant_dynamic-update-slice_fusion.5
  7.9 0.7 constant_dynamic-update-slice_fusion.4
  8.6 0.7 constant_dynamic-update-slice_fusion.3
  9.3 0.7 constant_dynamic-update-slice_fusion.2
  10.1 0.7 constant_dynamic-update-slice_fusion.1
  10.8 0.7 constant_dynamic-update-slice_fusion
  11.5 0.6 copy-done
  12.1 0.0 all-gather.9.cloned.1.call-update
  12.1 0.0 all-gather.11.cloned.1.call-start
  12.2 1.3 pad_maximum_fusion.1
  13.5 0.0 all-gather.11.cloned.1.call-update
  13.6 1.0 fusion.57
  14.6 0.8 slice_bitcast_fusion.15
  15.4 1.0 fusion.59
  16.4 8.4 %all-gather = bf16[32,2048]{1,0:T(8,128)(2,1)S(1)} all-gather(bf16[16,2048]{1,0:T(8,128)(2,1)S(1)} %get-tuple-element.164), channel_id=2, replica_groups=mesh['sp_0'=8,'sp_1'=8,'tp_0'=4,'tp_1'=2] {'tp_1'}, dimensions={0}, use_global_device_ids=true | all-gather | bytes 196608 | tf_op jit(solution)/shard_map/all_gather | solution.py:34
  24.8 9.4 %all-gather.1 = bf16[64,2048]{1,0:T(8,128)(2,1)S(1)} all-gather(bf16[16,2048]{1,0:T(8,128)(2,1)S(1)} %get-tuple-element.165), channel_id=3, replica_groups=mesh['sp_0'=8,'sp_1'=8,'tp_0'=4,'tp_1'=2] {'tp_0'}, dimensions={0}, use_global_device_ids=true | all-gather | bytes 327680 | tf_op jit(solution)/shard_map/all_gather | solution.py:34
  34.2 5.2 %all_gather.33 = bf16[8,16,2048]{2,1,0:T(8,128)(2,1)S(1)} all-gather(bf16[4,16,2048]{2,1,0:T(8,128)(2,1)S(1)} %bitcast.267), channel_id=1, replica_groups=mesh['sp_0'=8,'sp_1'=8,'tp_0'=4,'tp_1'=2] {'tp_1'}, dimensions={0}, use_global_device_ids=true | all-gather | bytes 786432 | tf_op jit(solution)/shard_map/all_gather | solution.py:34
  39.4 10.3 %all_gather.31 = bf16[8,16,2048]{2,1,0:T(8,128)(2,1)S(1)} all-gather(bf16[2,16,2048]{2,1,0:T(8,128)(2,1)S(1)} %bitcast.270), channel_id=1, replica_groups=mesh['sp_0'=8,'sp_1'=8,'tp_0'=4,'tp_1'=2] {'tp_0'}, dimensions={0}, use_global_device_ids=true | all-gather | bytes 655360 | tf_op jit(solution)/shard_map/all_gather | solution.py:34
  49.7 0.1 pad_maximum_fusion
  49.8 49.8 %all-gather.9.cloned.1.call-done = bf16[2048,896]{1,0:T(8,128)(2,1)} async-done(((bf16[32,896]{1,0:T(8,128)(2,1)}), bf16[2048,896]{1,0:T(8,128)(2,1)}) %all-gather.9.cloned.1.call-update) | async-done | bytes 3670032 | tf_op jit(solution)/shard_map/all_gather | solution.py:23
  99.6 1.5 convolution_convert_fusion
  101.1 1.5 convolution_convert_fusion.1
  102.5 0.0 copy-start.3
  102.6 0.0 copy-start.4
  102.6 2.7 %collective-permute-start = (bf16[2,2,128]{2,1,0:T(2,128)(2,1)S(1)}, bf16[2,2,128]{2,1,0:T(2,128)(2,1)S(1)}, u32[]{:S(2)}, u32[]{:S(2)}) collective-permute-start(bf16[2,2,128]{2,1,0:T(2,128)(2,1)S(1)} %pad_maximum_fusion.2), channel_id=1, source_target_pairs={{0,8},{8,16},{16,24},{24,32},{32,40},{40,48},{48,56},{56,64},{64,7... | collective-permute-start | bytes 3080 | tf_op jit(solution)/shard_map/ppermute | solution.py:100
  105.3 1.5 convolution_convert_fusion.5
  106.8 1.5 divide_multiply_fusion
  108.3 0.0 copy-done.3
  108.3 1.5 log-plus-one_add_fusion
  109.8 9.0 %while.17 = (s32[]{:T(128)}, f32[1,128,128]{2,1,0:T(8,128)S(1)}, f32[1,128]{1,0:T(1,128)S(1)}, f32[4,1,64,128]{3,2,1,0:T(8,128)S(1)}, f32[4,1,64,128]{3,2,1,0:T(...) while((s32[]{:T(128)}, f32[1,128,128]{2,1,0:T(8,128)S(1)}, ...), condition=%wide.region_4.5_spmd.clone, body=%wide.region_1.4_spmd.clone.sunk | while | flops 35234048 | bytes 983196 | solution.py:172
  109.9 0.1 reduce_window_sum.16
  110.0 0.2 fusion.178
  110.2 0.3 fusion.176
  110.5 1.3 multiply_reduce_fusion.3
  111.9 0.2 fusion.181
  112.1 0.1 reduce_window_sum.16
  112.2 0.2 fusion.178
  112.4 0.3 fusion.176
  112.8 1.3 multiply_reduce_fusion.3
  114.1 0.2 fusion.181
  114.3 0.1 reduce_window_sum.16
  114.5 0.2 fusion.178
  114.7 0.3 fusion.176
  115.0 1.3 multiply_reduce_fusion.3
  116.3 0.2 fusion.181
  116.6 0.1 reduce_window_sum.16
  116.7 0.2 fusion.178
  116.9 0.3 fusion.176
  117.2 1.3 multiply_reduce_fusion.3
  118.6 0.2 fusion.181
  118.8 0.0 copy-start.2
  118.8 0.0 copy-start.1
  118.8 21.1 %all-gather.4 = f32[8,129,128]{2,1,0:T(8,128)S(1)} all-gather(f32[1,129,128]{2,1,0:T(8,128)S(1)} %maximum_bitcast_fusion), channel_id=4, replica_groups=mesh['sp_0'=8,'sp_1'=8,'tp_0'=4,'tp_1'=2] {'sp_1'}, dimensions={0}, use_global_device_ids=true | all-gather | bytes 594432 | tf_op jit(solution)/shard_map/all_gather | solution.py:73
  139.9 0.2 slice_add_fusion.8
  140.1 19.0 %all-gather.5 = f32[8,129,128]{2,1,0:T(8,128)S(1)} all-gather(f32[1,129,128]{2,1,0:T(8,128)S(1)} %maximum_bitcast_fusion.1), channel_id=5, replica_groups=mesh['sp_0'=8,'sp_1'=8,'tp_0'=4,'tp_1'=2] {'sp_0'}, dimensions={0}, use_global_device_ids=true | all-gather | bytes 594432 | tf_op jit(solution)/shard_map/all_gather | solution.py:73
  159.2 0.7 multiply_reduce_fusion.1
  159.9 21.4 %all-gather.11.cloned.1.call-done = bf16[2048,256]{1,0:T(8,128)(2,1)} async-done(((bf16[32,256]{1,0:T(8,128)(2,1)}), bf16[2048,256]{1,0:T(8,128)(2,1)}) %all-gather.11.cloned.1.call-update) | async-done | bytes 1048592 | tf_op jit(solution)/shard_map/all_gather | solution.py:106
  181.3 2.0 fusion.51
  183.3 0.0 collective-permute-done
  183.4 3.0 %fusion.34 = bf16[256,2048]{1,0:T(8,128)(2,1)} fusion(f32[256,2048]{1,0:T(8,128)S(1)} %fusion.51, bf16[256,2048]{1,0:T(8,128)(2,1)S(1)} %bitcast.262, bf16[2048,256]{1,0:T(8,128)(2,1)} %all-gather.11.cloned.1.call-done, bf16[2048,896]{1,0:T(8,128)(2,1)} %all-gather.9.cloned.1.call-done, f32[258,128]{1,0:T(8,128)S(1)} %convert_multiply_fusion.2, ...), kind=kOutput, calls=%fused_computation.45 | convolution fusion | flops 269778944 | bytes 5637632 | tf_op jit(solution)/shard_map/dot_general | solution.py:265
  186.4 24.3 %all_to_all.5 = bf16[8,32,2048]{2,1,0:T(8,128)(2,1)S(1)} all-to-all(bf16[8,32,2048]{2,1,0:T(8,128)(2,1)} %bitcast.264), channel_id=1, replica_groups=mesh['sp_0'=8,'sp_1'=8,'tp_0'=4,'tp_1'=2] {'tp_0','tp_1'}, dimensions={0} | all-to-all | bytes 2097152 | tf_op jit(solution)/shard_map/all_to_all | solution.py:121
  210.7 0.8 reduce_sum.41
  (53 shorter events, 0.5 us)
Async XLA Ops:
  6.5 93.1 %all-gather.9.cloned.1.call-start = ((), (), s32[]{:S(2)}) async-start(), calls=%async_computation.1 | async-start | bytes 3727360 | tf_op jit(solution)/shard_map/all_gather | solution.py:23
  11.5 0.6 copy-start
  12.1 169.2 %all-gather.11.cloned.1.call-start = ((), (), s32[]{:S(2)}) async-start(), calls=%async_computation.2 | async-start | bytes 1064960 | tf_op jit(solution)/shard_map/all_gather | solution.py:106
  102.5 5.7 %copy-start.3 = (f32[256,1]{0,1:T(1,128)S(1)}, f32[256,1]{0,1:T(1,128)}, u32[]{:S(2)}) copy-start(f32[256,1]{0,1:T(1,128)} %param.28) | copy-start | bytes 3076
  102.6 5.7 %copy-start.4 = (f32[1,128]{1,0:T(1,128)S(1)}, f32[1,128]{1,0:T(1,128)}, u32[]{:S(2)}) copy-start(f32[1,128]{1,0:T(1,128)} %param.27) | copy-start | bytes 1540
  102.6 80.7 %collective-permute-start = (bf16[2,2,128]{2,1,0:T(2,128)(2,1)S(1)}, bf16[2,2,128]{2,1,0:T(2,128)(2,1)S(1)}, u32[]{:S(2)}, u32[]{:S(2)}) collective-permute-start(bf16[2,2,128]{2,1,0:T(2,128)(2,1)S(1)} %pad_maximum_fusion.2), channel_id=1, source_target_pairs={{0,8},{8,16},{16,24},{24,32},{32,40},{40,48},{48,56},{56,64},{64,7... | collective-permute-start | bytes 3080 | tf_op jit(solution)/shard_map/ppermute | solution.py:100
  118.8 40.4 %copy-start.2 = (f32[1,128,128]{2,1,0:T(8,128)S(1)}, f32[1,128,128]{2,1,0:T(8,128)}, u32[]{:S(2)}) copy-start(f32[1,128,128]{2,1,0:T(8,128)} %param.29) | copy-start | bytes 196612
  118.8 62.5 %copy-start.1 = (f32[128]{0:T(128)S(1)}, f32[128]{0:T(128)}, u32[]{:S(2)}) copy-start(f32[128]{0:T(128)} %param.30) | copy-start | bytes 1540
Sparse Core Ops, SparseCore 0:
  12.2 87.3 all-gather.8
  102.7 78.5 all-gather.10
where the time goes:
time: 219 us; the launch traced here: 218 us
  blocking collectives  97.5 us (45%)
  waiting for transfers between devices  71.2 us (33%)
  matrix products  15.7 us (7%)
  between operations  13.7 us (6%)
  other arithmetic  10.4 us (5%)
  local copies, waits for them, and re-layouts  6.58 us (3%)
  starting transfers between devices  2.76 us (1%)
    all_gather x1, waiting for transfers between devices, side_by_side(): lax.all_gather(both, axis, axis=dim, tiled=True)  49.8 us
    all_gather x2, blocking collectives, all_in_one(): both, at, found = (lax.all_gather(jnp.concatenate(lines), axis), 0, {})  40.1 us
    all_gather x4, blocking collectives, stacked_from(): parts = lax.all_gather(parts, axes[k], axis=0, tiled=True)  33.2 us
    all_to_all x1, blocking collectives, sum_at_owner(): lax.all_to_all(parts, axis, split_axis=0, concat_axis=0, tiled=True)  24.3 us
    all_gather x1, waiting for transfers between devices, turned_gather(): whole, at, done = (lax.all_gather(both, axis, axis=0, tiled=True), 0, [])  21.4 us
    dot_general x5, matrix products, project(): jnp.dot(shard_rows, matrix, preferred_element_type=jnp.float32)  7.36 us
    reduce_sum x4, other arithmetic, advance(): jnp.sum(query_block[:, :, None, :] * write_blk[:, None, :, :] * decays, a...  5.29 us
    unnamed x16, local copies, waits for them, and re-layouts  4.86 us
  transfers between devices with their start and end apart: 3, of which 2 were waited for; matrix products, arithmetic and copies ran while one was open for 11% of the time, Pallas kernels for 0%

commit v1 on v0

v1 whole, which is shorter than its diff:
```python
import functools

import jax
import jax.numpy as jnp
from jax import lax
from jax.experimental import pallas as pl
from jax.experimental.pallas import tpu as pltpu
from jax.sharding import Mesh
from jax.sharding import PartitionSpec as P

BLOCK = 64
Z, Y, X, C = "sp_0", "sp_1", "tp_0", "tp_1"
SP = (Z, Y)
TP = (X, C)
SP_TP = (Z, Y, X, C)
MESH = pl.DeviceIdType.MESH
EPS = 1e-06
HIGHEST = lax.Precision.HIGHEST
F32 = jnp.float32
BF16 = jnp.bfloat16


def dot(a, b, dims, precision=None):
    return lax.dot_general(a, b, (dims, ((), ())), precision=precision, preferred_element_type=F32)


def silu(v):
    return v * jax.nn.sigmoid(v)


def kernel(
    sizes,
    tokens,
    gain,
    w_query,
    w_forget,
    w_input,
    w_outgate,
    w_bgate,
    w_cgate,
    w_value,
    floor_gap,
    extra_decay,
    start_state,
    state_gain,
    taps,
    out_t,
    out,
    tok,
    wg0,
    wg1,
    wg2,
    wg3,
    wg4,
    normed_ref,
    lk_ref,
    r_ref,
    u_ref,
    w_ref,
    lprev,
    startt,
    ysend,
    yrecv,
    zbuf,
    pref,
    dec,
    back_send,
    back_recv,
    halo_send,
    gext,
    both,
    psend,
    precv,
    ssum,
    xrecv,
    load_sem,
    tokload_sem,
    p1_send,
    p1_recv,
    r_send,
    r_recv,
    tx_send,
    tx_recv,
    td_send,
    td_recv,
    st_send,
    st_recv,
    pd_send,
    pd_recv,
    px_send,
    px_recv,
):
    nz, ny, nx, nc = sizes
    z, y, x, c = (lax.axis_index(name) for name in (Z, Y, X, C))
    groups = (wg0, wg1, wg2, wg3, wg4)
    sources = (
        (w_forget, w_input),
        (w_query, w_outgate),
        (w_cgate, w_value),
        (w_bgate,),
        (out_t,),
    )
    half = tokens.shape[0] // 2
    rows = nx * nc * tokens.shape[0]
    blocks = rows // BLOCK
    dk = floor_gap.shape[1]
    vrows = dk // ny

    tok_load = pltpu.make_async_copy(tokens, tok.at[x, c], tokload_sem)
    tok_load.start()
    for g, parts in enumerate(sources):
        lo = 0
        for part in parts:
            width = part.shape[1]
            for h in range(2):
                pltpu.make_async_copy(
                    part.at[pl.ds(h * half, half)],
                    groups[g].at[z, y, h, :, pl.ds(lo, width)],
                    load_sem.at[g],
                ).start()
            lo += width

    wrap = jnp.where(y == ny - 1, 1, 0)
    unwrap = jnp.where(y == 0, 1, 0)
    after = {Z: lax.rem(z + wrap, nz), Y: lax.rem(y + 1, ny)}
    before = {Z: lax.rem(z + nz - unwrap, nz), Y: lax.rem(y + ny - 1, ny)}
    peers = [{Y: lax.rem(y + d, ny)} for d in range(1, ny)]
    peers += [{Z: lax.rem(z + d, nz)} for d in range(1, nz)]
    peers += [{X: lax.rem(x + d, nx)} for d in range(1, nx)]
    peers += [{C: 1 - c}, after, before]
    barrier = pltpu.get_barrier_semaphore()
    for peer in peers:
        pl.semaphore_signal(barrier, inc=1, device_id=peer, device_id_type=MESH)
    pl.semaphore_wait(barrier, len(peers))

    def remote(src, dst, send, recv, to):
        return pltpu.make_async_remote_copy(
            src_ref=src, dst_ref=dst, send_sem=send, recv_sem=recv, device_id=to, device_id_type=MESH
        )

    pending = []

    def ship(src, dst, send, recv, to):
        copy = remote(src, dst, send, recv, to)
        copy.start()
        pending.append(copy)

    def arrived(ref, send, recv, to):
        remote(ref, ref, send, recv, to).wait_recv()

    nkx = nx // 2

    def tok_ref(direction, k):
        index = lax.rem(x - direction * k + nx, nx)
        if k < nkx:
            return tok.at[index, c]
        lo = 0 if direction > 0 else half
        return tok.at[index, c, pl.ds(lo, half)]

    def tok_ship(direction, k):
        index = lax.rem(x - direction * (k - 1) + nx, nx)
        if k < nkx:
            ref = tok.at[index, c]
        else:
            ref = tok.at[index, c, pl.ds(0 if direction > 0 else half, half)]
        d = 0 if direction > 0 else 1
        to = {X: lax.rem(x + direction + nx, nx)}
        ship(ref, ref, tx_send.at[d, k - 1], tx_recv.at[d, k - 1], to)

    def tok_wait(direction, k):
        d = 0 if direction > 0 else 1
        arrived(
            tok_ref(direction, k),
            tx_send.at[d, k - 1],
            tx_recv.at[d, k - 1],
            {X: lax.rem(x + direction + nx, nx)},
        )

    def tok_across(offset):
        index = lax.rem(x + offset + nx, nx)
        ref = tok.at[index, c]
        at = offset % nx
        ship(ref, ref, td_send.at[at], td_recv.at[at], {C: 1 - c})

    def tok_across_wait(offset):
        index = lax.rem(x + offset + nx, nx)
        ref = tok.at[index, 1 - c]
        at = offset % nx
        arrived(ref, td_send.at[at], td_recv.at[at], {C: 1 - c})

    def first_hop(g):
        w = groups[g]
        for color, (axis, me, n) in enumerate(((Y, y, ny), (Z, z, nz))):
            ref = w.at[z, y, color]
            order = sorted(range(1, n), key=lambda d: -min(d, n - d))
            for d in order:
                remote(
                    ref, ref, p1_send.at[g, color], p1_recv.at[g, color], {axis: lax.rem(me + d, n)}
                ).start()

    def first_ref(g, color):
        w = groups[g]
        if color == 0:
            return w.at[z, pl.ds(0, ny - 1), 0]
        return w.at[pl.ds(0, nz - 1), y, 1]

    def first_wait(g):
        for color, axis in enumerate((Y, Z)):
            ref = first_ref(g, color)
            remote(
                ref, ref, p1_send.at[g, color], p1_recv.at[g, color], {axis: 0}
            ).wait_recv()

    def first_drain(g):
        for color, axis in enumerate((Y, Z)):
            ref = first_ref(g, color)
            remote(
                ref, ref, p1_send.at[g, color], p1_recv.at[g, color], {axis: 0}
            ).wait_send()

    rings = ((Z, z, nz), (Y, y, ny))

    def ring_ref(g, color, direction, k, last):
        axis, me, n = rings[color]
        index = lax.rem(me - direction * k + n, n)
        w = groups[g]
        other = (ny, nz)[color]
        if last:
            part = pl.ds(0 if direction > 0 else other // 2, other // 2)
        else:
            part = pl.ds(0, other)
        if color == 0:
            return w.at[index, part, 0]
        return w.at[part, index, 1]

    def ring_ship(g, k):
        for color in range(2):
            axis, me, n = rings[color]
            if k > n // 2:
                continue
            for d, direction in enumerate((1, -1)):
                ref = ring_ref(g, color, direction, k - 1, k == n // 2)
                ship(
                    ref,
                    ref,
                    r_send.at[g, color, d, k - 1],
                    r_recv.at[g, color, d, k - 1],
                    {axis: lax.rem(me + direction + n, n)},
                )

    def ring_wait(g, k):
        for color in range(2):
            axis, me, n = rings[color]
            if k > n // 2:
                continue
            for d, direction in enumerate((1, -1)):
                ref = ring_ref(g, color, direction, k, k == n // 2)
                arrived(
                    ref,
                    r_send.at[g, color, d, k - 1],
                    r_recv.at[g, color, d, k - 1],
                    {axis: lax.rem(me + direction + n, n)},
                )

    steps = max(nz, ny) // 2

    def front(i):
        for g in range(len(groups)):
            k = i - g + 1
            if k == 1:
                first_wait(g)
                ring_ship(g, 1)
            elif 2 <= k <= steps:
                ring_wait(g, k - 1)
                ring_ship(g, k)
            elif k == steps + 1:
                ring_wait(g, steps)

    def whole(g):
        w = groups[g][...]
        return w.reshape(-1, w.shape[-1])

    def wait_load(g):
        ref = groups[g].at[z, y]
        pltpu.make_async_copy(ref, ref, load_sem.at[g]).wait()

    wait_load(0)
    first_hop(0)
    tok_load.wait()
    for direction in (1, -1):
        tok_ship(direction, 1)
    tok_across(0)
    for g in range(1, len(groups)):
        wait_load(g)
        first_hop(g)
    startt[...] = start_state[0].T.reshape(startt.shape)

    front(0)
    for k in range(1, nkx + 1):
        for direction in (1, -1):
            tok_wait(direction, k)
            if k < nkx:
                tok_ship(direction, k + 1)
                tok_across(-direction * k)
    tok_across(nkx)
    front(1)
    for offset in range(nx):
        tok_across_wait(offset)
    front(2)
    tokens_f = tok[...].reshape(rows, tok.shape[-1]).astype(F32)
    scale = lax.rsqrt(jnp.mean(tokens_f * tokens_f, axis=-1, keepdims=True) + EPS)
    normed_ref[...] = (tokens_f * scale * gain[...]).astype(BF16)

    def project(g):
        raw = dot(normed_ref[...], whole(g), ((1,), (0,)))
        return raw.astype(BF16).astype(F32)

    row = lax.broadcasted_iota(jnp.int32, (BLOCK, BLOCK), 0)
    col = lax.broadcasted_iota(jnp.int32, (BLOCK, BLOCK), 1)
    causal = row >= col
    lower = causal.astype(F32)

    front(3)
    front(4)
    raw = project(0)
    write_in = floor_gap[...] * jax.nn.sigmoid(-raw[:, :dk])
    log_keep = jnp.log1p(-write_in) + extra_decay[...]
    w_ref[...] = write_in
    u_ref[...] = raw[:, dk:]
    memory = None
    total = jnp.zeros((1, dk), F32)
    for b in range(blocks):
        at = pl.ds(b * BLOCK, BLOCK)
        lk = log_keep[b * BLOCK : (b + 1) * BLOCK]
        running = dot(lower, lk, ((1,), (0,)), HIGHEST)
        r_ref[at] = running
        final = running[BLOCK - 1 :]
        lk_ref[pl.ds(b, 1)] = total
        total = total + final
        weighted = w_ref[at] * jnp.exp(final - running)
        fresh = dot(u_ref[at], weighted, ((0,), (0,)), HIGHEST)
        if memory is None:
            lprev[b] = jnp.zeros_like(fresh)
            memory = fresh
        else:
            lprev[b] = memory
            memory = memory * jnp.exp(final) + fresh
    ysend[:, pl.ds(0, vrows)] = memory.reshape(ny, vrows, dk)
    ysend[:, pl.ds(vrows, 8)] = jnp.broadcast_to(total[None], (ny, 8, dk))
    yrecv[y, pl.ds(0, vrows)] = ysend[y, pl.ds(0, vrows)]
    yrecv[y, pl.ds(vrows, 8)] = ysend[y, pl.ds(vrows, 8)]
    front(5)
    for d in range(1, ny):
        to = lax.rem(y + d, ny)
        remote(ysend.at[to], yrecv.at[y], st_send.at[0], st_recv.at[0], {Y: to}).start()

    raw = project(1)
    queries = silu(raw[:, :dk])
    gate_out = silu(raw[:, dk:])
    local, lifted = [], []
    for b in range(blocks):
        at = pl.ds(b * BLOCK, BLOCK)
        running = r_ref[at]
        mid = running[BLOCK // 2 - 1 : BLOCK // 2]
        q = queries[b * BLOCK : (b + 1) * BLOCK]
        scores = dot(
            q * jnp.exp(running - mid), w_ref[at] * jnp.exp(mid - running), ((1,), (1,)), HIGHEST
        )
        scores = jnp.where(causal, scores, 0.0)
        here = dot(scores, u_ref[at], ((1,), (0,)), HIGHEST)
        here = here + dot(q * jnp.exp(running), lprev[b], ((1,), (1,)), HIGHEST)
        local.append(here)
        lifted.append(q * jnp.exp(running + lk_ref[pl.ds(b, 1)]))
    local = jnp.concatenate(local, axis=0)
    lifted = jnp.concatenate(lifted, axis=0)

    front(6)
    ybytes = yrecv.at[pl.ds(0, ny - 1)]
    remote(ybytes, ybytes, st_send.at[0], st_recv.at[0], {Y: 0}).wait()
    so_far = jnp.zeros((vrows, dk), F32)
    logs = jnp.zeros((1, dk), F32)
    for j in range(ny):
        pref[j] = so_far
        dec[pl.ds(j, 1)] = logs
        step = yrecv[j, pl.ds(vrows, 1)]
        so_far = so_far * jnp.exp(step) + yrecv[j, pl.ds(0, vrows)]
        logs = logs + step
    zbuf[z, pl.ds(0, vrows)] = so_far
    zbuf[z, pl.ds(vrows, 8)] = jnp.broadcast_to(logs, (8, dk))

    raw = project(2)
    gated = raw[:, :dk] * raw[:, dk:]
    gext[pl.ds(8, rows)] = gated
    halo_send[...] = gated[rows - 8 :]
    for d in range(1, nz):
        ref = zbuf.at[z]
        remote(ref, ref, st_send.at[1], st_recv.at[1], {Z: lax.rem(z + d, nz)}).start()
    front(7)
    ship(halo_send, gext.at[pl.ds(0, 8)], st_send.at[3], st_recv.at[3], after)
    raw = project(3)
    zbytes = zbuf.at[pl.ds(0, nz - 1)]
    remote(zbytes, zbytes, st_send.at[1], st_recv.at[1], {Z: 0}).wait()
    carry = startt[y]
    for j in range(nz):
        later = carry * jnp.exp(zbuf[j, pl.ds(vrows, 1)]) + zbuf[j, pl.ds(0, vrows)]
        carry = jnp.where(j < z, later, carry)
    for j in range(ny):
        back_send[j] = carry * jnp.exp(dec[pl.ds(j, 1)]) + pref[j]
    back_recv[y] = back_send[y]

    arrived(gext.at[pl.ds(0, 8)], st_send.at[3], st_recv.at[3], after)
    first = jnp.logical_and(z == 0, y == 0)
    halo = jnp.where(first, 0.0, gext[pl.ds(0, 8)])
    gext[pl.ds(0, 8)] = halo
    conv = (
        taps[pl.ds(0, 1)] * gext[pl.ds(6, rows)]
        + taps[pl.ds(1, 1)] * gext[pl.ds(7, rows)]
        + taps[pl.ds(2, 1)] * gext[pl.ds(8, rows)]
    )
    short = (raw * conv).astype(BF16)
    both[:, :, :, pl.ds(dk, dk)] = short.reshape(nx, nc, rows // (nx * nc), dk)
    for d in range(1, ny):
        to = lax.rem(y + d, ny)
        remote(back_send.at[to], back_recv.at[y], st_send.at[2], st_recv.at[2], {Y: to}).start()
    front(8)
    bbytes = back_recv.at[pl.ds(0, ny - 1)]
    remote(bbytes, bbytes, st_send.at[2], st_recv.at[2], {Y: 0}).wait()
    carried = back_recv[...].reshape(dk, dk)
    mixed = local + dot(lifted, carried, ((1,), (1,)), HIGHEST)
    norm = lax.rsqrt(jnp.mean(mixed * mixed, axis=-1, keepdims=True) + EPS)
    rec = (mixed * norm * state_gain[...] * gate_out).astype(BF16)
    both[:, :, :, pl.ds(0, dk)] = rec.reshape(nx, nc, rows // (nx * nc), dk)

    per = rows // (nx * nc)
    weights = whole(4)
    width = out.shape[1]
    chunks = 4
    size = width // chunks
    theirs = both[:, 1 - c].reshape(nx * per, 2 * dk)
    mine = both[:, c].reshape(nx * per, 2 * dk)
    for q in range(chunks):
        at = pl.ds(q * size, size)
        part = dot(theirs, weights[q * size : (q + 1) * size], ((1,), (1,)))
        psend[:, :, at] = part.astype(BF16).reshape(nx, per, size)
        if q > 0:
            last = pl.ds((q - 1) * size, size)
            ship(psend.at[:, :, last], precv.at[:, :, last], pd_send.at[q - 1], pd_recv.at[q - 1], {C: 1 - c})
    own = [dot(mine, weights[q * size : (q + 1) * size], ((1,), (1,))) for q in range(chunks)]
    last = pl.ds((chunks - 1) * size, size)
    ship(psend.at[:, :, last], precv.at[:, :, last], pd_send.at[chunks - 1], pd_recv.at[chunks - 1], {C: 1 - c})

    def push(q):
        at = pl.ds(q * size, size)
        for d in range(1, nx):
            to = lax.rem(x + d, nx)
            ship(ssum.at[to, :, at], xrecv.at[x, :, at], px_send.at[q, d - 1], px_recv.at[q, d - 1], {X: to})

    for q in range(chunks):
        at = pl.ds(q * size, size)
        arrived(precv.at[:, :, at], pd_send.at[q], pd_recv.at[q], {C: 1 - c})
        mix = own[q].reshape(nx, per, size) + precv[:, :, at].astype(F32)
        ssum[:, :, at] = mix.astype(BF16)
        if q > 0:
            push(q - 1)
    push(chunks - 1)
    for q in range(chunks):
        at = pl.ds(q * size, size)
        acc = ssum[x, :, at].astype(F32)
        for d in range(1, nx):
            src = lax.rem(x + nx - d, nx)
            arrived(xrecv.at[src, :, at], px_send.at[q, d - 1], px_recv.at[q, d - 1], {X: src})
            acc = acc + xrecv[src, :, at].astype(F32)
        out[:, at] = acc.astype(BF16)

    for g in range(len(groups)):
        first_drain(g)
    for copy in pending:
        copy.wait_send()


def on_device(sizes, *args):
    (
        tokens,
        norm_gain,
        w_query,
        w_forget,
        w_input,
        w_outgate,
        w_bgate,
        w_cgate,
        w_value,
        floor_gap,
        extra_decay,
        start_state,
        state_gain,
        conv_taps,
        out_rec,
        out_conv,
    ) = args
    nz, ny, nx, nc = sizes
    per, model = tokens.shape
    rows = per * nx * nc
    blocks = rows // BLOCK
    dk = floor_gap.shape[1]
    half = per // 2
    vrows = dk // ny
    out_t = jnp.concatenate([out_rec.T, out_conv.T], axis=1)
    vmem = pl.BlockSpec(memory_space=pltpu.VMEM)
    hbm = pl.BlockSpec(memory_space=pl.ANY)
    dma = pltpu.SemaphoreType.DMA
    steps = max(nz, ny) // 2
    gathered = [(nz, ny, 2, half, k * dk) for k in (2, 2, 2, 1, 2)]
    scratch = [
        pltpu.VMEM((nx, nc, per, model), BF16),
        *[pltpu.VMEM(shape, BF16) for shape in gathered],
        pltpu.VMEM((rows, model), BF16),
        pltpu.VMEM((blocks, dk), F32),
        pltpu.VMEM((rows, dk), F32),
        pltpu.VMEM((rows, dk), F32),
        pltpu.VMEM((rows, dk), F32),
        pltpu.VMEM((blocks, dk, dk), F32),
        pltpu.VMEM((ny, vrows, dk), F32),
        pltpu.VMEM((ny, vrows + 8, dk), F32),
        pltpu.VMEM((ny, vrows + 8, dk), F32),
        pltpu.VMEM((nz, vrows + 8, dk), F32),
        pltpu.VMEM((ny, vrows, dk), F32),
        pltpu.VMEM((ny, dk), F32),
        pltpu.VMEM((ny, vrows, dk), F32),
        pltpu.VMEM((ny, vrows, dk), F32),
        pltpu.VMEM((8, dk), F32),
        pltpu.VMEM((rows + 8, dk), F32),
        pltpu.VMEM((nx, nc, per, 2 * dk), BF16),
        *[pltpu.VMEM((nx, per, model), BF16)] * 4,
        dma((5,)),
        dma,
        dma((5, 2)),
        dma((5, 2)),
        dma((5, 2, 2, steps)),
        dma((5, 2, 2, steps)),
        dma((2, nx // 2)),
        dma((2, nx // 2)),
        dma((nx,)),
        dma((nx,)),
        dma((4,)),
        dma((4,)),
        dma((4,)),
        dma((4,)),
        dma((4, nx - 1)),
        dma((4, nx - 1)),
    ]
    return pl.pallas_call(
        functools.partial(kernel, sizes),
        out_shape=jax.ShapeDtypeStruct((per, model), BF16),
        in_specs=[hbm, vmem] + [hbm] * 7 + [vmem] * 5 + [hbm],
        out_specs=vmem,
        scratch_shapes=scratch,
        compiler_params=pltpu.CompilerParams(collective_id=0, has_side_effects=True),
    )(
        tokens,
        norm_gain[None],
        w_query,
        w_forget,
        w_input,
        w_outgate,
        w_bgate,
        w_cgate,
        w_value,
        floor_gap,
        extra_decay,
        start_state,
        state_gain[None],
        conv_taps,
        out_t,
    )


def on_torus(devices, sizes):
    torus = Mesh(devices.reshape(sizes), SP_TP)
    return jax.shard_map(
        functools.partial(on_device, sizes),
        mesh=torus,
        in_specs=(
            P(SP_TP, None),
            P(),
            P(SP, TP),
            P(SP, TP),
            P(SP, TP),
            P(SP, TP),
            P(SP, TP),
            P(SP, TP),
            P(SP, TP),
            P(TP, None),
            P(SP, TP),
            P(TP, None, None),
            P(),
            P(None, TP),
            P(TP, SP),
            P(TP, SP),
        ),
        out_specs=P(SP_TP, None),
        check_vma=False,
    )


def solution(mesh):
    return on_torus(mesh.devices, (8, 8, 4, 2))
```

time: 219 us -> 82.4 us (0.38)
  blocking collectives: 97.5 us -> 0 us
  Pallas kernels: 0 us -> 78.5 us
  waiting for transfers between devices: 71.2 us -> 0 us
  matrix products: 15.7 us -> 0 us
  between operations: 13.7 us -> 0.01 us
  other arithmetic: 10.4 us -> 1.32 us
  local copies, waits for them, and re-layouts: 6.58 us -> 2.37 us
  starting transfers between devices: 2.76 us -> 0 us
    pallas_call x0 -> x1, Pallas kernels: none -> 78.5 us  [on_device(): pl.pallas_call(functools.partial(kernel, sizes), out_shape=jax.ShapeDtype...]
    all_gather x6 -> x0, blocking collectives: 73.3 us -> none  [the longest x2 40.1 us: all_in_one(): both, at, found = (lax.all_gather(jnp.concatenate(lines), axis), 0, {})]
    all_gather x2 -> x0, waiting for transfers between devices: 71.2 us -> none  [the longest x1 49.8 us: side_by_side(): lax.all_gather(both, axis, axis=dim, tiled=True)]
    all_to_all x1 -> x0, blocking collectives: 24.3 us -> none  [sum_at_owner(): lax.all_to_all(parts, axis, split_axis=0, concat_axis=0, tiled=True)]
    dot_general x20 -> x0, matrix products: 15.7 us -> none  [the longest x5 7.36 us: project(): jnp.dot(shard_rows, matrix, preferred_element_type=jnp.float32)]
    reduce_sum x6 -> x0, other arithmetic: 7.15 us -> none  [the longest x4 5.29 us: advance(): jnp.sum(query_block[:, :, None, :] * write_blk[:, None, :, :] * decays, a...]
    ppermute x1 -> x0, starting transfers between devices: 2.72 us -> none  [shifted(): return lax.ppermute(block, axis, route)]
    unnamed x16 -> x4, local copies, waits for them, and re-layouts: 4.86 us -> 2.37 us
  transfers between devices with their start and end apart: 3 -> 0, of which waited for: 2 -> 0; matrix products, arithmetic and copies ran while one was open for 11% -> 0% of each run, Pallas kernels for 0% -> 0%
where the time goes in v1:
time: 82.4 us; the launch traced here: 82.2 us
  Pallas kernels  78.5 us (95%)
  local copies, waits for them, and re-layouts  2.37 us (3%)
  other arithmetic  1.32 us (2%)
    pallas_call x1, Pallas kernels, on_device(): pl.pallas_call(functools.partial(kernel, sizes), out_shape=jax.ShapeDtype...  78.5 us
    unnamed x4, local copies, waits for them, and re-layouts  2.37 us

profile of v1, /device:TPU:1, one launch (start us, length us, event | category | flops | bytes accessed | tf_op | source)
XLA Modules:
  0.0 82.2 jit_solution(16071997415169540875)
XLA Ops:
  0.0 0.0 copy-start
  0.0 1.3 %pad_maximum_fusion.out_t = bf16[32,256]{1,0:T(8,128)(2,1)} fusion(bf16[32,128]{1,0:T(8,128)(2,1)} %bitcast.5, bf16[32,128]{1,0:T(8,128)(2,1)} %bitcast.6), kind=kLoop, calls=%fused_computation | loop fusion | flops 32768 | bytes 32768 | tf_op jit(solution)/shard_map/concatenate | solution.py:507
  1.3 0.0 copy-done
  1.3 0.8 copy.17.extra_decay
  2.1 78.5 %shard_map.154 = bf16[32,2048]{1,0:T(8,128)(2,1)} custom-call(bf16[32,2048]{1,0:T(8,128)(2,1)} %tokens.1, f32[1,2048]{1,0:T(1,128)} %bitcast.4, bf16[32,128]{1,0:T(8,128)(2,1)} %w_query.1, bf16[32,128]{1,0:T(8,128)(2,1)} %w_forget.1, bf16[32,128]{1,0:T(8,128)(2,1)} %w_input.1, bf16[32,128]{1,0:T(8,128)(2,1)} %w_outgate.1, bf16[32,128]{1,0:T(8,128)(2,1)} %w_bgate.1, ...), custom_call_target="tpu_custom_call" | custom-call | tf_op jit(solution)/shard_map/pallas_call | solution.py:551
  80.7 1.6 %copy.19 = bf16[32,2048]{1,0:T(8,128)(2,1)} copy(bf16[32,2048]{1,0:T(8,128)(2,1)} %shard_map.154) | data formatting | bytes 262144
Async XLA Ops:
  0.0 1.3 %copy-start = (f32[256,1]{0,1:T(1,128)S(1)}, f32[256,1]{0,1:T(1,128)}, u32[]{:S(2)}) copy-start(f32[256,1]{0,1:T(1,128)} %param.26) | copy-start | bytes 3076

commit v2 on v1

v2 whole, which is shorter than its diff:
```python
import functools

import jax
import jax.numpy as jnp
from jax import lax
from jax.experimental import pallas as pl
from jax.experimental.pallas import tpu as pltpu
from jax.sharding import Mesh
from jax.sharding import PartitionSpec as P

BLOCK = 64
Z, Y, X, C = "sp_0", "sp_1", "tp_0", "tp_1"
SP = (Z, Y)
TP = (X, C)
SP_TP = (Z, Y, X, C)
MESH = pl.DeviceIdType.MESH
EPS = 1e-06
HIGHEST = lax.Precision.HIGHEST
F32 = jnp.float32
BF16 = jnp.bfloat16


def dot(a, b, dims, precision=None):
    return lax.dot_general(a, b, (dims, ((), ())), precision=precision, preferred_element_type=F32)


def silu(v):
    return v * jax.nn.sigmoid(v)


def kernel(
    sizes,
    tokens,
    gain,
    w_query,
    w_forget,
    w_input,
    w_outgate,
    w_bgate,
    w_cgate,
    w_value,
    floor_gap,
    extra_decay,
    start_state,
    state_gain,
    taps,
    rec_t,
    conv_t,
    out,
    tok,
    wg0,
    wg1,
    wg2,
    wg3,
    wg4,
    wg5,
    normed_ref,
    off_ref,
    r_ref,
    u_ref,
    w_ref,
    lprev,
    startt,
    ysend,
    yrecv,
    zbuf,
    pref,
    dec,
    back_send,
    back_recv,
    halo_send,
    gext,
    both,
    psend,
    precv,
    ssum,
    xrecv,
    gain_v,
    gap_v,
    extra_v,
    start_v,
    sgain_v,
    taps_v,
    load_sem,
    p1_send,
    p1_recv,
    p1r_recv,
    r_send,
    r_recv,
    tx_send,
    tx_recv,
    td_send,
    td_recv,
    st_send,
    st_recv,
    pd_send,
    pd_recv,
    px_send,
    px_recv,
):
    nz, ny, nx, nc = sizes
    n = nz
    z, y, x, c = (lax.axis_index(name) for name in (Z, Y, X, C))
    groups = (wg0, wg1, wg2, wg3, wg4, wg5)
    sources = (
        (w_forget,),
        (w_input,),
        (w_query, w_outgate),
        (w_cgate, w_value),
        (w_bgate,),
        (rec_t, conv_t),
    )
    direct, relayed = (0, 1, 2), (3, 4, 5)
    half = tokens.shape[0] // 2
    rows = nx * nc * tokens.shape[0]
    blocks = rows // BLOCK
    dk = floor_gap.shape[1]
    vrows = dk // ny

    wrap = jnp.where(y == ny - 1, 1, 0)
    unwrap = jnp.where(y == 0, 1, 0)
    after = {Z: lax.rem(z + wrap, nz), Y: lax.rem(y + 1, ny)}
    before = {Z: lax.rem(z + nz - unwrap, nz), Y: lax.rem(y + ny - 1, ny)}
    far_first = sorted(range(1, n), key=lambda d: -min(d, n - d))
    peers = [{Y: lax.rem(y + d, ny)} for d in far_first]
    peers += [{Z: lax.rem(z + d, nz)} for d in far_first]
    peers += [{X: lax.rem(x + d, nx)} for d in range(1, nx)]
    peers += [{C: 1 - c}, after, before]
    barrier = pltpu.get_barrier_semaphore()
    for peer in peers:
        pl.semaphore_signal(barrier, inc=1, device_id=peer, device_id_type=MESH)

    tok_load = pltpu.make_async_copy(tokens, tok.at[x, c], load_sem.at[6])

    def load(g):
        lo = 0
        for part in sources[g]:
            width = part.shape[1]
            for h in range(2):
                pltpu.make_async_copy(
                    part.at[pl.ds(h * half, half)],
                    groups[g].at[z, y, h, :, pl.ds(lo, width)],
                    load_sem.at[g],
                ).start()
            lo += width

    def wait_load(g):
        ref = groups[g].at[z, y]
        pltpu.make_async_copy(ref, ref, load_sem.at[g]).wait()

    load(0)
    load(1)
    tok_load.start()
    for g in range(2, 6):
        load(g)
    small = [
        pltpu.make_async_copy(src, dst, load_sem.at[7 + i])
        for i, (src, dst) in enumerate(
            (
                (gain, gain_v),
                (floor_gap, gap_v),
                (extra_decay, extra_v),
                (start_state, start_v),
                (state_gain, sgain_v),
                (taps, taps_v),
            )
        )
    ]
    for copy in small:
        copy.start()
    for g in range(6):
        wait_load(g)
    tok_load.wait()
    pl.semaphore_wait(barrier, len(peers))

    def remote(src, dst, send, recv, to):
        return pltpu.make_async_remote_copy(
            src_ref=src, dst_ref=dst, send_sem=send, recv_sem=recv, device_id=to, device_id_type=MESH
        )

    pending = []

    def ship(src, dst, send, recv, to):
        copy = remote(src, dst, send, recv, to)
        copy.start()
        pending.append(copy)

    def landed(ref, recv):
        remote(ref, ref, recv, recv, {C: 1 - c}).wait_recv()

    def left(ref, send):
        remote(ref, ref, send, send, {C: 1 - c}).wait_send()

    nkx = nx // 2

    def tok_part(index, direction, k):
        if k < nkx:
            return tok.at[index, c]
        return tok.at[index, c, pl.ds(0 if direction > 0 else half, half)]

    def tok_ship(direction, k):
        ref = tok_part(lax.rem(x - direction * (k - 1) + nx, nx), direction, k)
        d = 0 if direction > 0 else 1
        to = {X: lax.rem(x + direction + nx, nx)}
        ship(ref, ref, tx_send.at[d, k - 1], tx_recv.at[d, k - 1], to)

    def tok_wait(direction, k):
        d = 0 if direction > 0 else 1
        landed(tok_part(lax.rem(x - direction * k + nx, nx), direction, k), tx_recv.at[d, k - 1])

    def tok_across(offset):
        ref = tok.at[lax.rem(x + offset + nx, nx), c]
        ship(ref, ref, td_send.at[offset % nx], td_recv.at[offset % nx], {C: 1 - c})

    def tok_across_wait(offset):
        landed(tok.at[lax.rem(x + offset + nx, nx), 1 - c], td_recv.at[offset % nx])

    lines = ((Y, y), (Z, z))

    def first_hop(g):
        for color, (axis, me) in enumerate(lines):
            ref = groups[g].at[z, y, color]
            for d in far_first:
                remote(
                    ref, ref, p1_send.at[g], p1_recv.at[g], {axis: lax.rem(me + d, n)}
                ).start()

    def first_wait(g):
        landed(groups[g].at[pl.ds(0, n - 1), 0], p1_recv.at[g])

    def relay_parts(k, direction):
        if k < n // 2:
            return relayed
        return relayed[:1] if direction > 0 else relayed[1:]

    def relay_ship(k):
        for color, (axis, me) in enumerate(lines):
            for direction in (1, -1):
                index = lax.rem(me - direction * (k - 1) + n, n)
                for g in relay_parts(k, direction):
                    w = groups[g]
                    ref = w.at[z, index, 0] if color == 0 else w.at[index, y, 1]
                    to = {axis: lax.rem(me + direction + n, n)}
                    remote(ref, ref, p1_send.at[g], p1r_recv.at[k - 1, g - 3], to).start()

    def relay_wait(k):
        for g in relayed:
            landed(groups[g].at[pl.ds(0, 2 if k < n // 2 else 1), 0], p1r_recv.at[k - 1, g - 3])

    rings = ((Z, z), (Y, y))
    steps = n // 2

    def ring_ship(g, k):
        w = groups[g]
        for color, (axis, me) in enumerate(rings):
            for direction in (1, -1):
                index = lax.rem(me - direction * (k - 1) + n, n)
                if k == steps:
                    part = pl.ds(0 if direction > 0 else n // 2, n // 2)
                else:
                    part = pl.ds(0, n)
                ref = w.at[index, part, 0] if color == 0 else w.at[part, index, 1]
                to = {axis: lax.rem(me + direction + n, n)}
                remote(ref, ref, r_send.at[g], r_recv.at[g, k - 1], to).start()

    def ring_wait(g, k):
        landed(groups[g].at[pl.ds(0, 2 if k < steps else 1)], r_recv.at[g, k - 1])

    sent, seen = [0] * 6, [0] * 6
    relayed_to = [0, 0]

    def see(g, k):
        while seen[g] < k:
            seen[g] += 1
            ring_wait(g, seen[g])

    def pass_on(k, *which):
        for g in which:
            while sent[g] < min(k, steps):
                see(g, sent[g])
                sent[g] += 1
                ring_ship(g, sent[g])

    def done(g):
        pass_on(steps, g)
        see(g, steps)

    def relay_on(k):
        while relayed_to[0] < min(k, steps):
            while relayed_to[1] < relayed_to[0]:
                relayed_to[1] += 1
                relay_wait(relayed_to[1])
            relayed_to[0] += 1
            relay_ship(relayed_to[0])

    def relay_done():
        relay_on(steps)
        relay_wait(steps)

    def whole(g):
        w = groups[g][...]
        return w.reshape(-1, w.shape[-1])

    def project(g):
        raw = dot(normed_ref[...], whole(g), ((1,), (0,)))
        return raw.astype(BF16).astype(F32)

    for g in direct[:2]:
        first_hop(g)
    for direction in (1, -1):
        tok_ship(direction, 1)
    tok_across(0)
    first_hop(2)
    relay_on(1)
    for copy in small:
        copy.wait()
    startt[...] = start_v[0].T.reshape(startt.shape)

    first_wait(0)
    pass_on(1, 0)
    first_wait(1)
    pass_on(1, 1)
    relay_on(2)
    for k in range(1, nkx):
        for direction in (1, -1):
            tok_wait(direction, k)
            tok_ship(direction, k + 1)
            tok_across(-direction * k)
    pass_on(2, 0, 1)
    first_wait(2)
    pass_on(1, 2)
    relay_on(3)
    for direction in (1, -1):
        tok_wait(direction, nkx)
    tok_across(nkx)
    pass_on(3, 0, 1)
    pass_on(2, 2)
    relay_on(4)
    for offset in range(nx):
        tok_across_wait(offset)
    tokens_f = tok[...].reshape(rows, tok.shape[-1]).astype(F32)
    scale = lax.rsqrt(jnp.mean(tokens_f * tokens_f, axis=-1, keepdims=True) + EPS)
    normed_ref[...] = (tokens_f * scale * gain_v[...]).astype(BF16)
    pass_on(4, 0, 1)
    relay_done()
    pass_on(1, 3)

    row = lax.broadcasted_iota(jnp.int32, (BLOCK, BLOCK), 0)
    col = lax.broadcasted_iota(jnp.int32, (BLOCK, BLOCK), 1)
    causal = row >= col
    lower = causal.astype(F32)

    done(0)
    raw = project(0)
    write_in = gap_v[...] * jax.nn.sigmoid(-raw)
    log_keep = jnp.log1p(-write_in)
    w_ref[...] = write_in
    done(1)
    u_ref[...] = project(1)
    memory = None
    total = jnp.zeros((1, dk), F32)
    for b in range(blocks):
        at = pl.ds(b * BLOCK, BLOCK)
        lk = log_keep[b * BLOCK : (b + 1) * BLOCK]
        extra = jnp.where(causal, extra_v[:, at], 0.0)
        running = dot(lower, lk, ((1,), (0,)), HIGHEST) + jnp.sum(extra, axis=1, keepdims=True)
        r_ref[at] = running
        final = running[BLOCK - 1 :]
        off_ref[pl.ds(b, 1)] = total
        total = total + final
        weighted = w_ref[at] * jnp.exp(final - running)
        fresh = dot(u_ref[at], weighted, ((0,), (0,)), HIGHEST)
        if memory is None:
            lprev[b] = jnp.zeros_like(fresh)
            memory = fresh
        else:
            lprev[b] = memory
            memory = memory * jnp.exp(final) + fresh
    ysend[:, pl.ds(0, vrows)] = memory.reshape(ny, vrows, dk)
    ysend[:, pl.ds(vrows, 8)] = jnp.broadcast_to(total[None], (ny, 8, dk))
    yrecv[y] = ysend[y]
    for d in far_first:
        to = lax.rem(y + d, ny)
        remote(ysend.at[to], yrecv.at[y], st_send.at[0], st_recv.at[0], {Y: to}).start()
    pass_on(1, 4, 5)
    pass_on(3, 2)
    pass_on(2, 3, 4, 5)
    pass_on(4, 2)

    done(2)
    raw = project(2)
    queries = silu(raw[:, :dk])
    gate_out = silu(raw[:, dk:])
    landed(yrecv.at[pl.ds(0, ny - 1)], st_recv.at[0])
    so_far = jnp.zeros((vrows, dk), F32)
    logs = jnp.zeros((1, dk), F32)
    for j in range(ny):
        pref[j] = so_far
        dec[pl.ds(j, 1)] = logs
        step = yrecv[j, pl.ds(vrows, 1)]
        so_far = so_far * jnp.exp(step) + yrecv[j, pl.ds(0, vrows)]
        logs = logs + step
    zbuf[z, pl.ds(0, vrows)] = so_far
    zbuf[z, pl.ds(vrows, 8)] = jnp.broadcast_to(logs, (8, dk))
    for d in far_first:
        ref = zbuf.at[z]
        remote(ref, ref, st_send.at[1], st_recv.at[1], {Z: lax.rem(z + d, nz)}).start()
    pass_on(3, 3, 4, 5)

    local, lifted = [], []
    for b in range(blocks):
        at = pl.ds(b * BLOCK, BLOCK)
        running = r_ref[at]
        mid = running[BLOCK // 2 - 1 : BLOCK // 2]
        q = queries[b * BLOCK : (b + 1) * BLOCK]
        scores = dot(
            q * jnp.exp(running - mid), w_ref[at] * jnp.exp(mid - running), ((1,), (1,)), HIGHEST
        )
        scores = jnp.where(causal, scores, 0.0)
        here = dot(scores, u_ref[at], ((1,), (0,)), HIGHEST)
        here = here + dot(q * jnp.exp(running), lprev[b], ((1,), (1,)), HIGHEST)
        local.append(here)
        lifted.append(q * jnp.exp(running + off_ref[pl.ds(b, 1)]))
    local = jnp.concatenate(local, axis=0)
    lifted = jnp.concatenate(lifted, axis=0)

    landed(zbuf.at[pl.ds(0, nz - 1)], st_recv.at[1])
    carry = startt[y]
    for j in range(nz):
        later = carry * jnp.exp(zbuf[j, pl.ds(vrows, 1)]) + zbuf[j, pl.ds(0, vrows)]
        carry = jnp.where(j < z, later, carry)
    for j in range(ny):
        back_send[j] = carry * jnp.exp(dec[pl.ds(j, 1)]) + pref[j]
    back_recv[y] = back_send[y]
    for d in far_first:
        to = lax.rem(y + d, ny)
        remote(back_send.at[to], back_recv.at[y], st_send.at[2], st_recv.at[2], {Y: to}).start()
    pass_on(4, 3, 4, 5)

    per = rows // (nx * nc)
    done(3)
    raw = project(3)
    gated = raw[:, :dk] * raw[:, dk:]
    gext[pl.ds(8, rows)] = gated
    halo_send[...] = gated[rows - 8 :]
    done(4)
    outer = project(4)
    ship(halo_send, gext.at[pl.ds(0, 8)], st_send.at[3], st_recv.at[3], after)
    landed(gext.at[pl.ds(0, 8)], st_recv.at[3])
    first = jnp.logical_and(z == 0, y == 0)
    halo = jnp.where(first, 0.0, gext[pl.ds(0, 8)])
    gext[pl.ds(0, 8)] = halo
    conv = (
        taps_v[pl.ds(0, 1)] * gext[pl.ds(6, rows)]
        + taps_v[pl.ds(1, 1)] * gext[pl.ds(7, rows)]
        + taps_v[pl.ds(2, 1)] * gext[pl.ds(8, rows)]
    )
    short = (outer * conv).astype(BF16)
    both[:, :, :, pl.ds(dk, dk)] = short.reshape(nx, nc, per, dk)

    landed(back_recv.at[pl.ds(0, ny - 1)], st_recv.at[2])
    carried = back_recv[...].reshape(dk, dk)
    mixed = local + dot(lifted, carried, ((1,), (1,)), HIGHEST)
    norm = lax.rsqrt(jnp.mean(mixed * mixed, axis=-1, keepdims=True) + EPS)
    rec = (mixed * norm * sgain_v[...] * gate_out).astype(BF16)
    both[:, :, :, pl.ds(0, dk)] = rec.reshape(nx, nc, per, dk)
    done(5)

    weights = whole(5)
    width = out.shape[1]
    chunks = 4
    size = width // chunks
    theirs = both[:, 1 - c].reshape(nx * per, 2 * dk)
    mine = both[:, c].reshape(nx * per, 2 * dk)

    def pair_ship(q):
        at = pl.ds(q * size, size)
        ship(psend.at[:, :, at], precv.at[:, :, at], pd_send.at[q], pd_recv.at[q], {C: 1 - c})

    own = []
    for q in range(chunks):
        part = dot(theirs, weights[q * size : (q + 1) * size], ((1,), (1,)))
        psend[:, :, pl.ds(q * size, size)] = part.astype(BF16).reshape(nx, per, size)
        own.append(dot(mine, weights[q * size : (q + 1) * size], ((1,), (1,))))
        pair_ship(q)

    def push(q):
        at = pl.ds(q * size, size)
        for d in range(1, nx):
            to = lax.rem(x + d, nx)
            ship(ssum.at[to, :, at], xrecv.at[x, :, at], px_send.at[q, d - 1], px_recv.at[q, d - 1], {X: to})

    for q in range(chunks):
        at = pl.ds(q * size, size)
        landed(precv.at[:, :, at], pd_recv.at[q])
        mix = own[q].reshape(nx, per, size) + precv[:, :, at].astype(F32)
        ssum[:, :, at] = mix.astype(BF16)
        if q > 0:
            push(q - 1)
    push(chunks - 1)
    for q in range(chunks):
        at = pl.ds(q * size, size)
        acc = ssum[x, :, at].astype(F32)
        for d in range(1, nx):
            src = lax.rem(x + nx - d, nx)
            landed(xrecv.at[src, :, at], px_recv.at[q, d - 1])
            acc = acc + xrecv[src, :, at].astype(F32)
        out[:, at] = acc.astype(BF16)

    for g in range(6):
        left(groups[g].at[pl.ds(0, n - 1), 0], p1_send.at[g])
        left(groups[g].at[pl.ds(0, n - 1)], r_send.at[g])
    left(ysend.at[pl.ds(0, ny - 1)], st_send.at[0])
    left(zbuf.at[pl.ds(0, nz - 1)], st_send.at[1])
    left(back_send.at[pl.ds(0, ny - 1)], st_send.at[2])
    for copy in pending:
        copy.wait_send()


def on_device(sizes, *args):
    (
        tokens,
        norm_gain,
        w_query,
        w_forget,
        w_input,
        w_outgate,
        w_bgate,
        w_cgate,
        w_value,
        floor_gap,
        extra_decay,
        start_state,
        state_gain,
        conv_taps,
        out_rec,
        out_conv,
    ) = args
    nz, ny, nx, nc = sizes
    per, model = tokens.shape
    rows = per * nx * nc
    blocks = rows // BLOCK
    dk = floor_gap.shape[1]
    half = per // 2
    vrows = dk // ny
    vmem = pl.BlockSpec(memory_space=pltpu.VMEM)
    hbm = pl.BlockSpec(memory_space=pl.ANY)
    dma = pltpu.SemaphoreType.DMA
    steps = nz // 2
    gathered = [(nz, ny, 2, half, k * dk) for k in (1, 1, 2, 2, 1, 2)]
    operands = (
        tokens,
        norm_gain[None],
        w_query,
        w_forget,
        w_input,
        w_outgate,
        w_bgate,
        w_cgate,
        w_value,
        floor_gap,
        extra_decay.T,
        start_state,
        state_gain[None],
        conv_taps,
        out_rec.T,
        out_conv.T,
    )
    small = (1, 9, 10, 11, 12, 13)
    scratch = [
        pltpu.VMEM((nx, nc, per, model), BF16),
        *[pltpu.VMEM(shape, BF16) for shape in gathered],
        pltpu.VMEM((rows, model), BF16),
        pltpu.VMEM((blocks, dk), F32),
        pltpu.VMEM((rows, dk), F32),
        pltpu.VMEM((rows, dk), F32),
        pltpu.VMEM((rows, dk), F32),
        pltpu.VMEM((blocks, dk, dk), F32),
        pltpu.VMEM((ny, vrows, dk), F32),
        pltpu.VMEM((ny, vrows + 8, dk), F32),
        pltpu.VMEM((ny, vrows + 8, dk), F32),
        pltpu.VMEM((nz, vrows + 8, dk), F32),
        pltpu.VMEM((ny, vrows, dk), F32),
        pltpu.VMEM((ny, dk), F32),
        pltpu.VMEM((ny, vrows, dk), F32),
        pltpu.VMEM((ny, vrows, dk), F32),
        pltpu.VMEM((8, dk), F32),
        pltpu.VMEM((rows + 8, dk), F32),
        pltpu.VMEM((nx, nc, per, 2 * dk), BF16),
        *[pltpu.VMEM((nx, per, model), BF16)] * 4,
        *[pltpu.VMEM(operands[i].shape, F32) for i in small],
        dma((13,)),
        dma((6,)),
        dma((3,)),
        dma((steps, 3)),
        dma((6,)),
        dma((6, steps)),
        dma((2, nx // 2)),
        dma((2, nx // 2)),
        dma((nx,)),
        dma((nx,)),
        dma((4,)),
        dma((4,)),
        dma((4,)),
        dma((4,)),
        dma((4, nx - 1)),
        dma((4, nx - 1)),
    ]
    return pl.pallas_call(
        functools.partial(kernel, sizes),
        out_shape=jax.ShapeDtypeStruct((per, model), BF16),
        in_specs=[hbm] * len(operands),
        out_specs=vmem,
        scratch_shapes=scratch,
        compiler_params=pltpu.CompilerParams(collective_id=0, has_side_effects=True),
    )(*operands)


def on_torus(devices, sizes):
    torus = Mesh(devices.reshape(sizes), SP_TP)
    return jax.shard_map(
        functools.partial(on_device, sizes),
        mesh=torus,
        in_specs=(
            P(SP_TP, None),
            P(),
            P(SP, TP),
            P(SP, TP),
            P(SP, TP),
            P(SP, TP),
            P(SP, TP),
            P(SP, TP),
            P(SP, TP),
            P(TP, None),
            P(SP, TP),
            P(TP, None, None),
            P(),
            P(None, TP),
            P(TP, SP),
            P(TP, SP),
        ),
        out_specs=P(SP_TP, None),
        check_vma=False,
    )


def solution(mesh):
    return on_torus(mesh.devices, (8, 8, 4, 2))
```

time: 82.4 us -> 77.3 us (0.938)
  Pallas kernels: 78.5 us -> 75.6 us
  other arithmetic: 1.32 us -> 0 us
    pallas_call x1, Pallas kernels: 78.5 us -> 75.6 us  [on_device(): pl.pallas_call(functools.partial(kernel, sizes), out_shape=jax.ShapeDtype...]
    concatenate x1 -> x0, other arithmetic: 1.32 us -> none  [on_device(): out_t = jnp.concatenate([out_rec.T, out_conv.T], axis=1)]
    unnamed x4 -> x1, local copies, waits for them, and re-layouts: 2.37 us -> 1.57 us
where the time goes in v2:
time: 77.3 us; the launch traced here: 77.2 us
  Pallas kernels  75.6 us (98%)
  local copies, waits for them, and re-layouts  1.57 us (2%)
    pallas_call x1, Pallas kernels, on_device(): pl.pallas_call(functools.partial(kernel, sizes), out_shape=jax.ShapeDtype...  75.6 us
    unnamed x1, local copies, waits for them, and re-layouts  1.57 us

profile of v2, /device:TPU:1, one launch (start us, length us, event | category | flops | bytes accessed | tf_op | source)
XLA Modules:
  0.0 77.2 jit_solution(17113178433149506856)
XLA Ops:
  0.0 75.6 %shard_map.154 = bf16[32,2048]{1,0:T(8,128)(2,1)} custom-call(bf16[32,2048]{1,0:T(8,128)(2,1)} %tokens.1, f32[1,2048]{1,0:T(1,128)} %bitcast.5, bf16[32,128]{1,0:T(8,128)(2,1)} %w_query.1, bf16[32,128]{1,0:T(8,128)(2,1)} %w_forget.1, bf16[32,128]{1,0:T(8,128)(2,1)} %w_input.1, bf16[32,128]{1,0:T(8,128)(2,1)} %w_outgate.1, bf16[32,128]{1,0:T(8,128)(2,1)} %w_bgate.1, ...), custom_call_target="tpu_custom_call" | custom-call | tf_op jit(solution)/shard_map/pallas_call | solution.py:609
  75.6 1.6 %copy.18 = bf16[32,2048]{1,0:T(8,128)(2,1)} copy(bf16[32,2048]{1,0:T(8,128)(2,1)} %shard_map.154) | data formatting | bytes 262144

commit v3 on v2

--- a/solution.py
+++ b/solution.py
@@ -74,6 +74,7 @@
     psend,
     precv,
     ssum,
+    xrelay,
     xrecv,
     gain_v,
     gap_v,
@@ -110,7 +111,6 @@
         (w_bgate,),
         (rec_t, conv_t),
     )
-    direct, relayed = (0, 1, 2), (3, 4, 5)
     half = tokens.shape[0] // 2
     rows = nx * nc * tokens.shape[0]
     blocks = rows // BLOCK
@@ -228,27 +228,43 @@
     def first_wait(g):
         landed(groups[g].at[pl.ds(0, n - 1), 0], p1_recv.at[g])
 
-    def relay_parts(k, direction):
-        if k < n // 2:
-            return relayed
-        return relayed[:1] if direction > 0 else relayed[1:]
+    relayed = (4, 5)
+    steps = n // 2
 
     def relay_ship(k):
         for color, (axis, me) in enumerate(lines):
             for direction in (1, -1):
                 index = lax.rem(me - direction * (k - 1) + n, n)
-                for g in relay_parts(k, direction):
+                to = {axis: lax.rem(me + direction + n, n)}
+                for g in relayed:
+                    if k == steps and (g == 4) == (direction > 0):
+                        continue
                     w = groups[g]
                     ref = w.at[z, index, 0] if color == 0 else w.at[index, y, 1]
-                    to = {axis: lax.rem(me + direction + n, n)}
-                    remote(ref, ref, p1_send.at[g], p1r_recv.at[k - 1, g - 3], to).start()
+                    remote(ref, ref, p1_send.at[g], p1r_recv.at[k - 1, g - 4], to).start()
 
     def relay_wait(k):
         for g in relayed:
-            landed(groups[g].at[pl.ds(0, 2 if k < n // 2 else 1), 0], p1r_recv.at[k - 1, g - 3])
+            landed(groups[g].at[pl.ds(0, 2 if k < steps else 1), 0], p1r_recv.at[k - 1, g - 4])
+
+    relay = [0, 0]
+
+    def relay_seen(k):
+        while relay[1] < k:
+            relay[1] += 1
+            relay_wait(relay[1])
+
+    def relay_on(k):
+        while relay[0] < min(k, steps):
+            relay_seen(relay[0])
+            relay[0] += 1
+            relay_ship(relay[0])
+
+    def relay_done():
+        relay_on(steps)
+        relay_seen(steps)
 
     rings = ((Z, z), (Y, y))
-    steps = n // 2
 
     def ring_ship(g, k):
         w = groups[g]
@@ -267,7 +283,6 @@
         landed(groups[g].at[pl.ds(0, 2 if k < steps else 1)], r_recv.at[g, k - 1])
 
     sent, seen = [0] * 6, [0] * 6
-    relayed_to = [0, 0]
 
     def see(g, k):
         while seen[g] < k:
@@ -285,18 +300,6 @@
         pass_on(steps, g)
         see(g, steps)
 
-    def relay_on(k):
-        while relayed_to[0] < min(k, steps):
-            while relayed_to[1] < relayed_to[0]:
-                relayed_to[1] += 1
-                relay_wait(relayed_to[1])
-            relayed_to[0] += 1
-            relay_ship(relayed_to[0])
-
-    def relay_done():
-        relay_on(steps)
-        relay_wait(steps)
-
     def whole(g):
         w = groups[g][...]
         return w.reshape(-1, w.shape[-1])
@@ -305,12 +308,13 @@
         raw = dot(normed_ref[...], whole(g), ((1,), (0,)))
         return raw.astype(BF16).astype(F32)
 
-    for g in direct[:2]:
-        first_hop(g)
+    first_hop(0)
+    first_hop(1)
     for direction in (1, -1):
         tok_ship(direction, 1)
     tok_across(0)
     first_hop(2)
+    first_hop(3)
     relay_on(1)
     for copy in small:
         copy.wait()
@@ -320,6 +324,8 @@
     pass_on(1, 0)
     first_wait(1)
     pass_on(1, 1)
+    first_wait(2)
+    pass_on(1, 2)
     relay_on(2)
     for k in range(1, nkx):
         for direction in (1, -1):
@@ -327,15 +333,16 @@
             tok_ship(direction, k + 1)
             tok_across(-direction * k)
     pass_on(2, 0, 1)
-    first_wait(2)
-    pass_on(1, 2)
     relay_on(3)
+    first_wait(3)
+    pass_on(2, 2)
+    pass_on(1, 3)
     for direction in (1, -1):
         tok_wait(direction, nkx)
     tok_across(nkx)
     pass_on(3, 0, 1)
-    pass_on(2, 2)
     relay_on(4)
+    pass_on(3, 2)
     for offset in range(nx):
         tok_across_wait(offset)
     tokens_f = tok[...].reshape(rows, tok.shape[-1]).astype(F32)
@@ -343,7 +350,9 @@
     normed_ref[...] = (tokens_f * scale * gain_v[...]).astype(BF16)
     pass_on(4, 0, 1)
     relay_done()
-    pass_on(1, 3)
+    pass_on(4, 2)
+    pass_on(1, 4, 5)
+    pass_on(2, 3)
 
     row = lax.broadcasted_iota(jnp.int32, (BLOCK, BLOCK), 0)
     col = lax.broadcasted_iota(jnp.int32, (BLOCK, BLOCK), 1)
@@ -379,19 +388,18 @@
     ysend[:, pl.ds(0, vrows)] = memory.reshape(ny, vrows, dk)
     ysend[:, pl.ds(vrows, 8)] = jnp.broadcast_to(total[None], (ny, 8, dk))
     yrecv[y] = ysend[y]
+    msg = pl.ds(0, vrows + 1)
     for d in far_first:
         to = lax.rem(y + d, ny)
-        remote(ysend.at[to], yrecv.at[y], st_send.at[0], st_recv.at[0], {Y: to}).start()
-    pass_on(1, 4, 5)
-    pass_on(3, 2)
-    pass_on(2, 3, 4, 5)
-    pass_on(4, 2)
+        remote(ysend.at[to, msg], yrecv.at[y, msg], st_send.at[0], st_recv.at[0], {Y: to}).start()
+    pass_on(2, 4, 5)
+    pass_on(3, 3)
 
     done(2)
     raw = project(2)
     queries = silu(raw[:, :dk])
     gate_out = silu(raw[:, dk:])
-    landed(yrecv.at[pl.ds(0, ny - 1)], st_recv.at[0])
+    landed(yrecv.at[pl.ds(0, ny - 1), msg], st_recv.at[0])
     so_far = jnp.zeros((vrows, dk), F32)
     logs = jnp.zeros((1, dk), F32)
     for j in range(ny):
@@ -403,9 +411,10 @@
     zbuf[z, pl.ds(0, vrows)] = so_far
     zbuf[z, pl.ds(vrows, 8)] = jnp.broadcast_to(logs, (8, dk))
     for d in far_first:
-        ref = zbuf.at[z]
+        ref = zbuf.at[z, msg]
         remote(ref, ref, st_send.at[1], st_recv.at[1], {Z: lax.rem(z + d, nz)}).start()
-    pass_on(3, 3, 4, 5)
+    pass_on(3, 4, 5)
+    pass_on(4, 3)
 
     local, lifted = [], []
     for b in range(blocks):
@@ -424,7 +433,17 @@
     local = jnp.concatenate(local, axis=0)
     lifted = jnp.concatenate(lifted, axis=0)
 
-    landed(zbuf.at[pl.ds(0, nz - 1)], st_recv.at[1])
+    per = rows // (nx * nc)
+    pass_on(4, 4)
+    done(3)
+    raw = project(3)
+    gated = raw[:, :dk] * raw[:, dk:]
+    gext[pl.ds(8, rows)] = gated
+    halo_send[...] = gated[rows - 8 :]
+    pass_on(4, 5)
+    ship(halo_send, gext.at[pl.ds(0, 8)], st_send.at[3], st_recv.at[3], after)
+
+    landed(zbuf.at[pl.ds(0, nz - 1), msg], st_recv.at[1])
     carry = startt[y]
     for j in range(nz):
         later = carry * jnp.exp(zbuf[j, pl.ds(vrows, 1)]) + zbuf[j, pl.ds(0, vrows)]
@@ -435,17 +454,16 @@
     for d in far_first:
         to = lax.rem(y + d, ny)
         remote(back_send.at[to], back_recv.at[y], st_send.at[2], st_recv.at[2], {Y: to}).start()
-    pass_on(4, 3, 4, 5)
-
-    per = rows // (nx * nc)
-    done(3)
-    raw = project(3)
-    gated = raw[:, :dk] * raw[:, dk:]
-    gext[pl.ds(8, rows)] = gated
-    halo_send[...] = gated[rows - 8 :]
+
     done(4)
     outer = project(4)
-    ship(halo_send, gext.at[pl.ds(0, 8)], st_send.at[3], st_recv.at[3], after)
+    landed(back_recv.at[pl.ds(0, ny - 1)], st_recv.at[2])
+    carried = back_recv[...].reshape(dk, dk)
+    mixed = local + dot(lifted, carried, ((1,), (1,)), HIGHEST)
+    norm = lax.rsqrt(jnp.mean(mixed * mixed, axis=-1, keepdims=True) + EPS)
+    rec = (mixed * norm * sgain_v[...] * gate_out).astype(BF16)
+    both[:, :, :, pl.ds(0, dk)] = rec.reshape(nx, nc, per, dk)
+
     landed(gext.at[pl.ds(0, 8)], st_recv.at[3])
     first = jnp.logical_and(z == 0, y == 0)
     halo = jnp.where(first, 0.0, gext[pl.ds(0, 8)])
@@ -457,13 +475,6 @@
     )
     short = (outer * conv).astype(BF16)
     both[:, :, :, pl.ds(dk, dk)] = short.reshape(nx, nc, per, dk)
-
-    landed(back_recv.at[pl.ds(0, ny - 1)], st_recv.at[2])
-    carried = back_recv[...].reshape(dk, dk)
-    mixed = local + dot(lifted, carried, ((1,), (1,)), HIGHEST)
-    norm = lax.rsqrt(jnp.mean(mixed * mixed, axis=-1, keepdims=True) + EPS)
-    rec = (mixed * norm * sgain_v[...] * gate_out).astype(BF16)
-    both[:, :, :, pl.ds(0, dk)] = rec.reshape(nx, nc, per, dk)
     done(5)
 
     weights = whole(5)
@@ -475,7 +486,7 @@
 
     def pair_ship(q):
         at = pl.ds(q * size, size)
-        ship(psend.at[:, :, at], precv.at[:, :, at], pd_send.at[q], pd_recv.at[q], {C: 1 - c})
+        remote(psend.at[:, :, at], precv.at[:, :, at], pd_send, pd_recv.at[q], {C: 1 - c}).start()
 
     own = []
     for q in range(chunks):
@@ -484,11 +495,29 @@
         own.append(dot(mine, weights[q * size : (q + 1) * size], ((1,), (1,))))
         pair_ship(q)
 
+    part = size // 2
+    ways = ((0, lax.rem(x + 1, nx)), (1, lax.rem(x + nx - 1, nx)))
+    opposite = lax.rem(x + nx // 2, nx)
+    relays = nx == 4
+
+    def hop(src, dst, q, kind, d, to):
+        remote(src, dst, px_send, px_recv.at[q, kind, d], {X: to}).start()
+
+    def cols(q, d):
+        return pl.ds(q * size + d * part, part)
+
+    def push_far(q):
+        if relays:
+            for d, to in ways:
+                hop(ssum.at[opposite, :, cols(q, d)], xrelay.at[:, cols(q, d)], q, 0, d, to)
+
     def push(q):
-        at = pl.ds(q * size, size)
-        for d in range(1, nx):
-            to = lax.rem(x + d, nx)
-            ship(ssum.at[to, :, at], xrecv.at[x, :, at], px_send.at[q, d - 1], px_recv.at[q, d - 1], {X: to})
+        for d, to in ways:
+            hop(ssum.at[to, :, cols(q, 1 - d)], xrecv.at[d, :, cols(q, 1 - d)], q, 1, d, to)
+
+    def push_added(q):
+        for d, to in ways:
+            hop(ssum.at[to, :, cols(q, d)], xrecv.at[d, :, cols(q, d)], q, 2, d, to)
 
     for q in range(chunks):
         at = pl.ds(q * size, size)
@@ -496,23 +525,41 @@
         mix = own[q].reshape(nx, per, size) + precv[:, :, at].astype(F32)
         ssum[:, :, at] = mix.astype(BF16)
         if q > 0:
-            push(q - 1)
-    push(chunks - 1)
+            push_far(q - 1)
+    push_far(chunks - 1)
+    for q in range(chunks):
+        push(q)
+    if relays:
+        for q in range(chunks):
+            for d, to in ways:
+                landed(xrelay.at[:, cols(q, d)], px_recv.at[q, 0, d])
+                added = ssum[to, :, cols(q, d)].astype(F32) + xrelay[:, cols(q, d)].astype(F32)
+                ssum[to, :, cols(q, d)] = added.astype(BF16)
+            if q > 0:
+                push_added(q - 1)
+        push_added(chunks - 1)
     for q in range(chunks):
         at = pl.ds(q * size, size)
         acc = ssum[x, :, at].astype(F32)
-        for d in range(1, nx):
-            src = lax.rem(x + nx - d, nx)
-            landed(xrecv.at[src, :, at], px_recv.at[q, d - 1])
-            acc = acc + xrecv[src, :, at].astype(F32)
+        for d, to in ways:
+            landed(xrecv.at[d, :, cols(q, 1 - d)], px_recv.at[q, 1, d])
+            if relays:
+                landed(xrecv.at[d, :, cols(q, d)], px_recv.at[q, 2, d])
+        if relays:
+            acc = acc + xrecv[0, :, at].astype(F32) + xrecv[1, :, at].astype(F32)
+        else:
+            ways_back = [xrecv[1 - h, :, cols(q, h)].astype(F32) for h in range(2)]
+            acc = acc + jnp.concatenate(ways_back, axis=1)
         out[:, at] = acc.astype(BF16)
 
     for g in range(6):
         left(groups[g].at[pl.ds(0, n - 1), 0], p1_send.at[g])
         left(groups[g].at[pl.ds(0, n - 1)], r_send.at[g])
-    left(ysend.at[pl.ds(0, ny - 1)], st_send.at[0])
-    left(zbuf.at[pl.ds(0, nz - 1)], st_send.at[1])
+    left(ysend.at[pl.ds(0, ny - 1), msg], st_send.at[0])
+    left(zbuf.at[pl.ds(0, nz - 1), msg], st_send.at[1])
     left(back_send.at[pl.ds(0, ny - 1)], st_send.at[2])
+    left(psend, pd_send)
+    left(ssum.at[pl.ds(0, nx - 1)], px_send)
     for copy in pending:
         copy.wait_send()
 
@@ -587,12 +634,14 @@
         pltpu.VMEM((8, dk), F32),
         pltpu.VMEM((rows + 8, dk), F32),
         pltpu.VMEM((nx, nc, per, 2 * dk), BF16),
-        *[pltpu.VMEM((nx, per, model), BF16)] * 4,
+        *[pltpu.VMEM((nx, per, model), BF16)] * 3,
+        pltpu.VMEM((per, model), BF16),
+        pltpu.VMEM((2, per, model), BF16),
         *[pltpu.VMEM(operands[i].shape, F32) for i in small],
         dma((13,)),
         dma((6,)),
-        dma((3,)),
-        dma((steps, 3)),
+        dma((6,)),
+        dma((steps, 2)),
         dma((6,)),
         dma((6, steps)),
         dma((2, nx // 2)),
@@ -601,10 +650,10 @@
         dma((nx,)),
         dma((4,)),
         dma((4,)),
+        dma,
         dma((4,)),
-        dma((4,)),
-        dma((4, nx - 1)),
-        dma((4, nx - 1)),
+        dma,
+        dma((4, 3, 2)),
     ]
     return pl.pallas_call(
         functools.partial(kernel, sizes),

time: 77.3 us -> 69.9 us (0.904)
  Pallas kernels: 75.6 us -> 68.2 us
    pallas_call x1, Pallas kernels: 75.6 us -> 68.2 us  [on_device(): pl.pallas_call(functools.partial(kernel, sizes), out_shape=jax.ShapeDtype...]
where the time goes in v3:
time: 69.9 us; the launch traced here: 69.8 us
  Pallas kernels  68.2 us (98%)
  local copies, waits for them, and re-layouts  1.57 us (2%)
    pallas_call x1, Pallas kernels, on_device(): pl.pallas_call(functools.partial(kernel, sizes), out_shape=jax.ShapeDtype...  68.2 us
    unnamed x1, local copies, waits for them, and re-layouts  1.57 us

profile of v3, /device:TPU:1, one launch (start us, length us, event | category | flops | bytes accessed | tf_op | source)
XLA Modules:
  0.0 69.8 jit_solution(13754819825832142799)
XLA Ops:
  0.0 68.2 %shard_map.154 = bf16[32,2048]{1,0:T(8,128)(2,1)} custom-call(bf16[32,2048]{1,0:T(8,128)(2,1)} %tokens.1, f32[1,2048]{1,0:T(1,128)} %bitcast.5, bf16[32,128]{1,0:T(8,128)(2,1)} %w_query.1, bf16[32,128]{1,0:T(8,128)(2,1)} %w_forget.1, bf16[32,128]{1,0:T(8,128)(2,1)} %w_input.1, bf16[32,128]{1,0:T(8,128)(2,1)} %w_outgate.1, bf16[32,128]{1,0:T(8,128)(2,1)} %w_bgate.1, ...), custom_call_target="tpu_custom_call" | custom-call | tf_op jit(solution)/shard_map/pallas_call | solution.py:658
  68.2 1.6 %copy.18 = bf16[32,2048]{1,0:T(8,128)(2,1)} copy(bf16[32,2048]{1,0:T(8,128)(2,1)} %shard_map.154) | data formatting | bytes 262144

commit v4 on v3

--- a/solution.py
+++ b/solution.py
@@ -63,7 +63,9 @@
     startt,
     ysend,
     yrecv,
+    ydec,
     zbuf,
+    zdec,
     pref,
     dec,
     back_send,
@@ -106,8 +108,8 @@
     sources = (
         (w_forget,),
         (w_input,),
+        (w_cgate, w_value),
         (w_query, w_outgate),
-        (w_cgate, w_value),
         (w_bgate,),
         (rec_t, conv_t),
     )
@@ -334,9 +336,7 @@
             tok_across(-direction * k)
     pass_on(2, 0, 1)
     relay_on(3)
-    first_wait(3)
     pass_on(2, 2)
-    pass_on(1, 3)
     for direction in (1, -1):
         tok_wait(direction, nkx)
     tok_across(nkx)
@@ -349,10 +349,11 @@
     scale = lax.rsqrt(jnp.mean(tokens_f * tokens_f, axis=-1, keepdims=True) + EPS)
     normed_ref[...] = (tokens_f * scale * gain_v[...]).astype(BF16)
     pass_on(4, 0, 1)
+    first_wait(3)
+    pass_on(1, 3)
     relay_done()
     pass_on(4, 2)
     pass_on(1, 4, 5)
-    pass_on(2, 3)
 
     row = lax.broadcasted_iota(jnp.int32, (BLOCK, BLOCK), 0)
     col = lax.broadcasted_iota(jnp.int32, (BLOCK, BLOCK), 1)
@@ -385,37 +386,70 @@
         else:
             lprev[b] = memory
             memory = memory * jnp.exp(final) + fresh
-    ysend[:, pl.ds(0, vrows)] = memory.reshape(ny, vrows, dk)
-    ysend[:, pl.ds(vrows, 8)] = jnp.broadcast_to(total[None], (ny, 8, dk))
+    ysend[...] = memory.reshape(ny, vrows, dk).astype(BF16)
+    ydec[y] = jnp.broadcast_to(total, (8, dk))
     yrecv[y] = ysend[y]
-    msg = pl.ds(0, vrows + 1)
+    line = pl.ds(0, 1)
     for d in far_first:
         to = lax.rem(y + d, ny)
-        remote(ysend.at[to, msg], yrecv.at[y, msg], st_send.at[0], st_recv.at[0], {Y: to}).start()
-    pass_on(2, 4, 5)
-    pass_on(3, 3)
-
+        remote(ysend.at[to], yrecv.at[y], st_send.at[0], st_recv.at[0], {Y: to}).start()
+        ref = ydec.at[y, line]
+        remote(ref, ref, st_send.at[4], st_recv.at[4], {Y: to}).start()
+    pass_on(2, 3, 4, 5)
+
+    per = rows // (nx * nc)
     done(2)
     raw = project(2)
-    queries = silu(raw[:, :dk])
-    gate_out = silu(raw[:, dk:])
-    landed(yrecv.at[pl.ds(0, ny - 1), msg], st_recv.at[0])
+    gated = raw[:, :dk] * raw[:, dk:]
+    gext[pl.ds(8, rows)] = gated
+    halo_send[...] = gated[rows - 8 :]
+
+    landed(yrecv.at[pl.ds(0, ny - 1)], st_recv.at[0])
+    landed(ydec.at[pl.ds(0, ny - 1), line], st_recv.at[4])
     so_far = jnp.zeros((vrows, dk), F32)
     logs = jnp.zeros((1, dk), F32)
     for j in range(ny):
         pref[j] = so_far
         dec[pl.ds(j, 1)] = logs
-        step = yrecv[j, pl.ds(vrows, 1)]
-        so_far = so_far * jnp.exp(step) + yrecv[j, pl.ds(0, vrows)]
+        step = ydec[j, line]
+        so_far = so_far * jnp.exp(step) + yrecv[j].astype(F32)
         logs = logs + step
-    zbuf[z, pl.ds(0, vrows)] = so_far
-    zbuf[z, pl.ds(vrows, 8)] = jnp.broadcast_to(logs, (8, dk))
+    zbuf[z] = so_far.astype(BF16)
+    zdec[z] = jnp.broadcast_to(logs, (8, dk))
     for d in far_first:
-        ref = zbuf.at[z, msg]
-        remote(ref, ref, st_send.at[1], st_recv.at[1], {Z: lax.rem(z + d, nz)}).start()
-    pass_on(3, 4, 5)
-    pass_on(4, 3)
-
+        for k, ref in ((1, zbuf.at[z]), (5, zdec.at[z, line])):
+            remote(ref, ref, st_send.at[k], st_recv.at[k], {Z: lax.rem(z + d, nz)}).start()
+    ship(halo_send, gext.at[pl.ds(0, 8)], st_send.at[3], st_recv.at[3], after)
+    pass_on(3, 3, 4, 5)
+    pass_on(4, 3, 4)
+
+    landed(zbuf.at[pl.ds(0, nz - 1)], st_recv.at[1])
+    landed(zdec.at[pl.ds(0, nz - 1), line], st_recv.at[5])
+    carry = startt[y]
+    for j in range(nz):
+        later = carry * jnp.exp(zdec[j, line]) + zbuf[j].astype(F32)
+        carry = jnp.where(j < z, later, carry)
+    for j in range(ny):
+        back_send[j] = (carry * jnp.exp(dec[pl.ds(j, 1)]) + pref[j]).astype(BF16)
+    back_recv[y] = back_send[y]
+    for d in far_first:
+        to = lax.rem(y + d, ny)
+        remote(back_send.at[to], back_recv.at[y], st_send.at[2], st_recv.at[2], {Y: to}).start()
+
+    pass_on(4, 5)
+    landed(gext.at[pl.ds(0, 8)], st_recv.at[3])
+    first = jnp.logical_and(z == 0, y == 0)
+    halo = jnp.where(first, 0.0, gext[pl.ds(0, 8)])
+    gext[pl.ds(0, 8)] = halo
+    conv = (
+        taps_v[pl.ds(0, 1)] * gext[pl.ds(6, rows)]
+        + taps_v[pl.ds(1, 1)] * gext[pl.ds(7, rows)]
+        + taps_v[pl.ds(2, 1)] * gext[pl.ds(8, rows)]
+    )
+    done(3)
+    raw = project(3)
+    queries = silu(raw[:, :dk])
+    gate_out = silu(raw[:, dk:])
     local, lifted = [], []
     for b in range(blocks):
         at = pl.ds(b * BLOCK, BLOCK)
@@ -433,48 +467,16 @@
     local = jnp.concatenate(local, axis=0)
     lifted = jnp.concatenate(lifted, axis=0)
 
-    per = rows // (nx * nc)
-    pass_on(4, 4)
-    done(3)
-    raw = project(3)
-    gated = raw[:, :dk] * raw[:, dk:]
-    gext[pl.ds(8, rows)] = gated
-    halo_send[...] = gated[rows - 8 :]
-    pass_on(4, 5)
-    ship(halo_send, gext.at[pl.ds(0, 8)], st_send.at[3], st_recv.at[3], after)
-
-    landed(zbuf.at[pl.ds(0, nz - 1), msg], st_recv.at[1])
-    carry = startt[y]
-    for j in range(nz):
-        later = carry * jnp.exp(zbuf[j, pl.ds(vrows, 1)]) + zbuf[j, pl.ds(0, vrows)]
-        carry = jnp.where(j < z, later, carry)
-    for j in range(ny):
-        back_send[j] = carry * jnp.exp(dec[pl.ds(j, 1)]) + pref[j]
-    back_recv[y] = back_send[y]
-    for d in far_first:
-        to = lax.rem(y + d, ny)
-        remote(back_send.at[to], back_recv.at[y], st_send.at[2], st_recv.at[2], {Y: to}).start()
-
     done(4)
-    outer = project(4)
+    short = (project(4) * conv).astype(BF16)
+    both[:, :, :, pl.ds(dk, dk)] = short.reshape(nx, nc, per, dk)
     landed(back_recv.at[pl.ds(0, ny - 1)], st_recv.at[2])
-    carried = back_recv[...].reshape(dk, dk)
+    carried = back_recv[...].reshape(dk, dk).astype(F32)
     mixed = local + dot(lifted, carried, ((1,), (1,)), HIGHEST)
     norm = lax.rsqrt(jnp.mean(mixed * mixed, axis=-1, keepdims=True) + EPS)
     rec = (mixed * norm * sgain_v[...] * gate_out).astype(BF16)
     both[:, :, :, pl.ds(0, dk)] = rec.reshape(nx, nc, per, dk)
 
-    landed(gext.at[pl.ds(0, 8)], st_recv.at[3])
-    first = jnp.logical_and(z == 0, y == 0)
-    halo = jnp.where(first, 0.0, gext[pl.ds(0, 8)])
-    gext[pl.ds(0, 8)] = halo
-    conv = (
-        taps_v[pl.ds(0, 1)] * gext[pl.ds(6, rows)]
-        + taps_v[pl.ds(1, 1)] * gext[pl.ds(7, rows)]
-        + taps_v[pl.ds(2, 1)] * gext[pl.ds(8, rows)]
-    )
-    short = (outer * conv).astype(BF16)
-    both[:, :, :, pl.ds(dk, dk)] = short.reshape(nx, nc, per, dk)
     done(5)
 
     weights = whole(5)
@@ -488,12 +490,13 @@
         at = pl.ds(q * size, size)
         remote(psend.at[:, :, at], precv.at[:, :, at], pd_send, pd_recv.at[q], {C: 1 - c}).start()
 
-    own = []
     for q in range(chunks):
         part = dot(theirs, weights[q * size : (q + 1) * size], ((1,), (1,)))
         psend[:, :, pl.ds(q * size, size)] = part.astype(BF16).reshape(nx, per, size)
-        own.append(dot(mine, weights[q * size : (q + 1) * size], ((1,), (1,))))
-        pair_ship(q)
+        if q > 0:
+            pair_ship(q - 1)
+    own = [dot(mine, weights[:size], ((1,), (1,)))]
+    pair_ship(chunks - 1)
 
     part = size // 2
     ways = ((0, lax.rem(x + 1, nx)), (1, lax.rem(x + nx - 1, nx)))
@@ -515,29 +518,32 @@
         for d, to in ways:
             hop(ssum.at[to, :, cols(q, 1 - d)], xrecv.at[d, :, cols(q, 1 - d)], q, 1, d, to)
 
-    def push_added(q):
-        for d, to in ways:
-            hop(ssum.at[to, :, cols(q, d)], xrecv.at[d, :, cols(q, d)], q, 2, d, to)
+    def push_added(q, way):
+        d, to = way
+        hop(ssum.at[to, :, cols(q, d)], xrecv.at[d, :, cols(q, d)], q, 2, d, to)
 
     for q in range(chunks):
         at = pl.ds(q * size, size)
         landed(precv.at[:, :, at], pd_recv.at[q])
         mix = own[q].reshape(nx, per, size) + precv[:, :, at].astype(F32)
         ssum[:, :, at] = mix.astype(BF16)
-        if q > 0:
-            push_far(q - 1)
-    push_far(chunks - 1)
+        if q < chunks - 1:
+            own.append(dot(mine, weights[(q + 1) * size : (q + 2) * size], ((1,), (1,))))
+        push_far(q)
     for q in range(chunks):
         push(q)
     if relays:
+        held = None
         for q in range(chunks):
-            for d, to in ways:
+            for way in ways:
+                d, to = way
                 landed(xrelay.at[:, cols(q, d)], px_recv.at[q, 0, d])
                 added = ssum[to, :, cols(q, d)].astype(F32) + xrelay[:, cols(q, d)].astype(F32)
                 ssum[to, :, cols(q, d)] = added.astype(BF16)
-            if q > 0:
-                push_added(q - 1)
-        push_added(chunks - 1)
+                if held is not None:
+                    push_added(*held)
+                held = (q, way)
+        push_added(*held)
     for q in range(chunks):
         at = pl.ds(q * size, size)
         acc = ssum[x, :, at].astype(F32)
@@ -555,8 +561,10 @@
     for g in range(6):
         left(groups[g].at[pl.ds(0, n - 1), 0], p1_send.at[g])
         left(groups[g].at[pl.ds(0, n - 1)], r_send.at[g])
-    left(ysend.at[pl.ds(0, ny - 1), msg], st_send.at[0])
-    left(zbuf.at[pl.ds(0, nz - 1), msg], st_send.at[1])
+    left(ysend.at[pl.ds(0, ny - 1)], st_send.at[0])
+    left(ydec.at[pl.ds(0, ny - 1), line], st_send.at[4])
+    left(zbuf.at[pl.ds(0, nz - 1)], st_send.at[1])
+    left(zdec.at[pl.ds(0, nz - 1), line], st_send.at[5])
     left(back_send.at[pl.ds(0, ny - 1)], st_send.at[2])
     left(psend, pd_send)
     left(ssum.at[pl.ds(0, nx - 1)], px_send)
@@ -624,13 +632,15 @@
         pltpu.VMEM((rows, dk), F32),
         pltpu.VMEM((blocks, dk, dk), F32),
         pltpu.VMEM((ny, vrows, dk), F32),
-        pltpu.VMEM((ny, vrows + 8, dk), F32),
-        pltpu.VMEM((ny, vrows + 8, dk), F32),
-        pltpu.VMEM((nz, vrows + 8, dk), F32),
+        pltpu.VMEM((ny, vrows, dk), BF16),
+        pltpu.VMEM((ny, vrows, dk), BF16),
+        pltpu.VMEM((ny, 8, dk), F32),
+        pltpu.VMEM((nz, vrows, dk), BF16),
+        pltpu.VMEM((nz, 8, dk), F32),
         pltpu.VMEM((ny, vrows, dk), F32),
         pltpu.VMEM((ny, dk), F32),
-        pltpu.VMEM((ny, vrows, dk), F32),
-        pltpu.VMEM((ny, vrows, dk), F32),
+        pltpu.VMEM((ny, vrows, dk), BF16),
+        pltpu.VMEM((ny, vrows, dk), BF16),
         pltpu.VMEM((8, dk), F32),
         pltpu.VMEM((rows + 8, dk), F32),
         pltpu.VMEM((nx, nc, per, 2 * dk), BF16),
@@ -648,8 +658,8 @@
         dma((2, nx // 2)),
         dma((nx,)),
         dma((nx,)),
-        dma((4,)),
-        dma((4,)),
+        dma((6,)),
+        dma((6,)),
         dma,
         dma((4,)),
         dma,

time: 69.9 us -> 64.8 us (0.927)
  Pallas kernels: 68.2 us -> 63.1 us
    pallas_call x1, Pallas kernels: 68.2 us -> 63.1 us  [on_device(): pl.pallas_call(functools.partial(kernel, sizes), out_shape=jax.ShapeDtype...]
where the time goes in v4:
time: 64.8 us; the launch traced here: 64.6 us
  Pallas kernels  63.1 us (97%)
  local copies, waits for them, and re-layouts  1.57 us (2%)
    pallas_call x1, Pallas kernels, on_device(): pl.pallas_call(functools.partial(kernel, sizes), out_shape=jax.ShapeDtype...  63.1 us
    unnamed x1, local copies, waits for them, and re-layouts  1.57 us

profile of v4, /device:TPU:1, one launch (start us, length us, event | category | flops | bytes accessed | tf_op | source)
XLA Modules:
  0.0 64.6 jit_solution(16664529656338110188)
XLA Ops:
  0.0 63.1 %shard_map.154 = bf16[32,2048]{1,0:T(8,128)(2,1)} custom-call(bf16[32,2048]{1,0:T(8,128)(2,1)} %tokens.1, f32[1,2048]{1,0:T(1,128)} %bitcast.5, bf16[32,128]{1,0:T(8,128)(2,1)} %w_query.1, bf16[32,128]{1,0:T(8,128)(2,1)} %w_forget.1, bf16[32,128]{1,0:T(8,128)(2,1)} %w_input.1, bf16[32,128]{1,0:T(8,128)(2,1)} %w_outgate.1, bf16[32,128]{1,0:T(8,128)(2,1)} %w_bgate.1, ...), custom_call_target="tpu_custom_call" | custom-call | tf_op jit(solution)/shard_map/pallas_call | solution.py:668
  63.1 1.6 %copy.18 = bf16[32,2048]{1,0:T(8,128)(2,1)} copy(bf16[32,2048]{1,0:T(8,128)(2,1)} %shard_map.154) | data formatting | bytes 262144

commit v5 on v4

--- a/solution.py
+++ b/solution.py
@@ -481,7 +481,7 @@
 
     weights = whole(5)
     width = out.shape[1]
-    chunks = 4
+    chunks = 8
     size = width // chunks
     theirs = both[:, 1 - c].reshape(nx * per, 2 * dk)
     mine = both[:, c].reshape(nx * per, 2 * dk)
@@ -661,9 +661,9 @@
         dma((6,)),
         dma((6,)),
         dma,
-        dma((4,)),
+        dma((8,)),
         dma,
-        dma((4, 3, 2)),
+        dma((8, 3, 2)),
     ]
     return pl.pallas_call(
         functools.partial(kernel, sizes),

time: 64.8 us -> 65.3 us (level)
  no operation moved by 1% of the time
where the time goes in v5:
time: 65.3 us; the launch traced here: 65.2 us
  Pallas kernels  63.6 us (97%)
  local copies, waits for them, and re-layouts  1.57 us (2%)
    pallas_call x1, Pallas kernels, on_device(): pl.pallas_call(functools.partial(kernel, sizes), out_shape=jax.ShapeDtype...  63.6 us
    unnamed x1, local copies, waits for them, and re-layouts  1.57 us

profile of v5, /device:TPU:1, one launch (start us, length us, event | category | flops | bytes accessed | tf_op | source)
XLA Modules:
  0.0 65.2 jit_solution(9243329622395914521)
XLA Ops:
  0.0 63.6 %shard_map.154 = bf16[32,2048]{1,0:T(8,128)(2,1)} custom-call(bf16[32,2048]{1,0:T(8,128)(2,1)} %tokens.1, f32[1,2048]{1,0:T(1,128)} %bitcast.5, bf16[32,128]{1,0:T(8,128)(2,1)} %w_query.1, bf16[32,128]{1,0:T(8,128)(2,1)} %w_forget.1, bf16[32,128]{1,0:T(8,128)(2,1)} %w_input.1, bf16[32,128]{1,0:T(8,128)(2,1)} %w_outgate.1, bf16[32,128]{1,0:T(8,128)(2,1)} %w_bgate.1, ...), custom_call_target="tpu_custom_call" | custom-call | tf_op jit(solution)/shard_map/pallas_call | solution.py:668
  63.6 1.6 %copy.18 = bf16[32,2048]{1,0:T(8,128)(2,1)} copy(bf16[32,2048]{1,0:T(8,128)(2,1)} %shard_map.154) | data formatting | bytes 262144
